TPU v7x, 32 devices: a whole 2x2x4 slice. The times are simulated.
32 devices in a mesh: sp: 8 (over z, y), tp: 4 (over x, core).
Axes of the slice: x: 2, y: 2, z: 4, core: 2. Of those that a mesh axis runs over, the one named last changes fastest.
Arguments:
- residual_entry_input: bfloat16 [8192, 2048], P(('sp', 'tp')), may hold values from -6 to 6
- query_matrix_rows: bfloat16 [8192, 1024], P('sp', 'tp'), may hold values from -6 to 6
- key_matrix_rows: bfloat16 [8192, 1024], P('sp', 'tp'), may hold values from -6 to 6
- value_matrix_rows: bfloat16 [8192, 2048], P('sp', 'tp'), may hold values from -6 to 6
- output_gate_logits: bfloat16 [8192, 2048], P('sp', 'tp'), may hold values from -6 to 6
- input_gate_logits: float32 [8192, 8], P('sp', 'tp'), may hold values from -6 to 6
- forget_gate_logits: float32 [8192, 8], P('sp', 'tp'), may hold values from -8 to 31
- forget_decay_offset: float32 [8192, 8], P('sp', 'tp'), may hold values from -0.7 to 0
- head_norm_gain: float32 [8, 256], P('tp'), may hold values from 0.1 to 1.9
- cell_output_weight: bfloat16 [2048, 2048], P('tp'), may hold values from -0.125 to 0.125
- feedforward_norm_gain: float32 [2048], replicated, may hold values from 0.1 to 1.9
- gate_up_weight: bfloat16 [2048, 5632], P('sp', 'tp'), may hold values from -0.125 to 0.125
- value_up_weight: bfloat16 [2048, 5632], P('sp', 'tp'), may hold values from -0.125 to 0.125
- gate_filter_taps: float32 [3, 5632], P(None, 'tp'), may hold values from -3 to 3
- value_filter_taps: float32 [3, 5632], P(None, 'tp'), may hold values from -3 to 3
- down_projection_weight: bfloat16 [5632, 2048], P('tp', 'sp'), may hold values from -0.078125 to 0.078125
Outputs:
- result: bfloat16 [8192, 2048], P(('sp', 'tp'))
All inputs are finite; a program needn't handle non-finite values.
Results may differ from a plain program's by a relative error of at most 0.025.
Values may be sent and summed in bfloat16 or wider, within the bound.
A program may use at most 128 MiB of HBM per device.

v0:
```python
import functools

import jax
import jax.numpy as jnp
from jax import lax
from jax.experimental import pallas as pl
from jax.experimental.pallas import tpu as pltpu
from jax.sharding import PartitionSpec as P

BLOCK = 128


eps = 1e-06
neg_large = -1e30


def shifted(x, axis, by):
    count = lax.axis_size(axis)
    pairs = [(i, i + by) for i in range(count) if 0 <= i + by < count]
    return lax.ppermute(x, axis, pairs)


def gate_log_values(input_gate_logits, forget_gate_logits, forget_decay_offset):
    input_log_value = 15.0 * jnp.tanh(input_gate_logits / 15.0)
    forget_log_sigmoid = (
        jax.nn.log_sigmoid(15.0 * jnp.tanh(forget_gate_logits / 15.0)) + forget_decay_offset
    )
    return (input_log_value, forget_log_sigmoid)


STATE_PAD = 16
MESH = pl.DeviceIdType.MESH


def cell_kernel(
    count,
    heads,
    state_ref,
    q_ref,
    k_ref,
    v_ref,
    gate_ref,
    gain_ref,
    rows_ref,
    cols_ref,
    out_ref,
    held,
    memory,
    normer,
    running,
    send_sem,
    recv_sem,
):
    me = lax.axis_index("sp")
    barrier = pltpu.get_barrier_semaphore()
    for d in range(1, count):
        pl.semaphore_signal(
            barrier, inc=1, device_id={"sp": lax.rem(me + d, count)}, device_id_type=MESH
        )
    pl.semaphore_wait(barrier, count - 1)

    def push(d, target, slot):
        return pltpu.make_async_remote_copy(
            src_ref=state_ref,
            dst_ref=held.at[slot],
            send_sem=send_sem.at[d],
            recv_sem=recv_sem.at[d],
            device_id={"sp": target},
            device_id_type=MESH,
        )

    for d in range(1, count):

        @pl.when(me + d < count)
        def _():
            push(d, me + d, me).start()

    memory[...] = jnp.zeros_like(memory)
    normer[...] = jnp.zeros_like(normer)
    running[...] = jnp.full(running.shape, neg_large, jnp.float32)
    for d in range(1, count):

        @pl.when(me - d >= 0)
        def _():
            push(d, lax.rem(me + d, count), me - d).wait_recv()

    key_width = memory.shape[1]
    value_width = memory.shape[2]
    span = key_width + STATE_PAD

    @pl.loop(0, me)
    def _(j):
        for h in range(heads):
            low = h * span
            extra = held[j, low + key_width : low + span, :].astype(jnp.float32)
            total = extra[2:3, :1] + extra[3:4, :1]
            level = extra[4:5, :1] + extra[5:6, :1]
            before = running[h, :1, :1]
            after = jnp.maximum(total + before, level)
            one = jnp.exp(total + before - after)
            two = jnp.exp(level - after)
            memory[h] = one * memory[h] + two * held[j, low : low + key_width, :].astype(
                jnp.float32
            )
            parts = extra[0:1, :key_width] + extra[1:2, :key_width]
            normer[h, :1, :] = one * normer[h, :1, :] + two * parts
            running[h] = jnp.broadcast_to(after, running.shape[1:])

    length = BLOCK
    scale = key_width ** (-0.5)
    at_row = lax.broadcasted_iota(jnp.int32, (length, length), 0)
    at_col = lax.broadcasted_iota(jnp.int32, (length, length), 1)
    causal = at_col <= at_row

    @pl.loop(0, q_ref.shape[0] // length)
    def _(j):
        rows = pl.ds(pl.multiple_of(j * length, length), length)
        lanes = rows_ref[j]
        cols = cols_ref[rows, :]
        for h in range(heads):
            keys = slice(h * key_width, (h + 1) * key_width)
            vals = slice(h * value_width, (h + 1) * value_width)
            q = q_ref[rows, keys]
            k = k_ref[rows, keys]
            v = v_ref[rows, vals]
            before = running[h, :1, :1]
            total = lanes[heads + h : heads + h + 1, :1]
            shifted_log = jnp.where(causal, lanes[h : h + 1, :], -jnp.inf)
            top = jnp.maximum(jnp.max(shifted_log, axis=1, keepdims=True), before)
            raw = (
                lax.dot_general(
                    q, k, (((1,), (1,)), ((), ())), preferred_element_type=jnp.float32
                )
                * scale
            )
            scores = raw * jnp.exp(shifted_log - top)
            carry = jnp.exp(before - top) * scale
            state = memory[h]
            high = state.astype(jnp.bfloat16)
            low = (state - high.astype(jnp.float32)).astype(jnp.bfloat16)
            carried = jnp.dot(q, high, preferred_element_type=jnp.float32) + jnp.dot(
                q, low, preferred_element_type=jnp.float32
            )
            numerator = carry * carried + jnp.dot(
                scores.astype(jnp.bfloat16), v, preferred_element_type=jnp.float32
            )
            denominator = carry * jnp.sum(
                q.astype(jnp.float32) * normer[h, :1, :], axis=1, keepdims=True
            ) + jnp.sum(scores, axis=1, keepdims=True)
            level = cols[:, h : h + 1] + top
            value = numerator / jnp.maximum(jnp.abs(denominator), jnp.exp(-level))
            mean = jnp.mean(value * value, axis=1, keepdims=True)
            normed = value * lax.rsqrt(mean + eps) * gain_ref[h : h + 1, :]
            gated = normed * jax.nn.sigmoid(gate_ref[rows, vals].astype(jnp.float32))
            out_ref[rows, vals] = gated.astype(out_ref.dtype)
            last = jnp.max(jnp.maximum(lanes[h : h + 1, :], before), axis=1, keepdims=True)
            decay = jnp.exp(before - last)
            weighted = k.astype(jnp.float32) * jnp.exp(cols[:, heads + h : heads + h + 1] - last)
            memory[h] = decay * state + lax.dot_general(
                weighted.astype(jnp.bfloat16),
                v,
                (((0,), (0,)), ((), ())),
                preferred_element_type=jnp.float32,
            )
            normer[h, :1, :] = decay * normer[h, :1, :] + jnp.sum(
                weighted, axis=0, keepdims=True
            )
            running[h] = jnp.broadcast_to(last + total, running.shape[1:])

    for d in range(1, count):

        @pl.when(me + d < count)
        def _():
            push(d, me + d, me).wait_send()


def halves(x):
    high = lax.reduce_precision(x, 8, 7)
    return (high.astype(jnp.bfloat16), (x - high).astype(jnp.bfloat16))


def cell(q, k, v, gates, input_log, forget_log, gain):
    heads = input_log.shape[1]
    tokens = q.shape[0]
    key_width = q.shape[1] // heads
    value_width = v.shape[1] // heads
    count = lax.axis_size("sp")
    blocks = tokens // BLOCK
    f = forget_log.reshape(blocks, BLOCK, heads)
    tri = jnp.tril(jnp.ones((BLOCK, BLOCK), jnp.float32))
    within = jnp.einsum("ts,bsh->bth", tri, f, precision=lax.Precision.HIGHEST)
    each = within[:, -1, :]
    later = jnp.triu(jnp.ones((blocks, blocks), jnp.float32), 1)
    after = jnp.einsum("bc,ch->bh", later, each, precision=lax.Precision.HIGHEST)
    total = jnp.sum(each, axis=0)
    shifted_log = input_log.reshape(blocks, BLOCK, heads) - within
    to_end = (shifted_log + (each + after)[:, None, :]).reshape(tokens, heads)
    level = jnp.max(to_end, axis=0)
    weighted = k.reshape(tokens, heads, key_width).astype(jnp.float32) * jnp.exp(to_end - level)[
        :, :, None
    ]
    memory = jnp.einsum(
        "shd,shv->hdv",
        weighted.astype(jnp.bfloat16),
        v.reshape(tokens, heads, value_width),
        preferred_element_type=jnp.float32,
    ).astype(jnp.bfloat16)
    normer = jnp.sum(weighted, axis=0)
    wide = (heads, 1, value_width)
    lines = [
        jnp.pad(part, ((0, 0), (0, value_width - key_width)))[:, None, :]
        for part in halves(normer)
    ]
    for scalar in (total, level):
        lines += [jnp.broadcast_to(part[:, None, None], wide) for part in halves(scalar)]
    lines.append(jnp.zeros((heads, STATE_PAD - len(lines), value_width), jnp.bfloat16))
    span = key_width + STATE_PAD
    state = jnp.concatenate([memory] + lines, axis=1).reshape(heads * span, value_width)
    lanes = jnp.concatenate(
        [
            jnp.transpose(shifted_log, (0, 2, 1)),
            jnp.broadcast_to(each[:, :, None], (blocks, heads, BLOCK)),
        ],
        axis=1,
    )
    cols = jnp.concatenate([within, shifted_log], axis=2).reshape(tokens, 2 * heads)
    vmem = pl.BlockSpec(memory_space=pltpu.VMEM)
    return pl.pallas_call(
        functools.partial(cell_kernel, count, heads),
        out_shape=jax.ShapeDtypeStruct(v.shape, jnp.bfloat16),
        in_specs=[vmem] * 8,
        out_specs=vmem,
        scratch_shapes=[
            pltpu.VMEM((count, heads * span, value_width), jnp.bfloat16),
            pltpu.VMEM((heads, key_width, value_width), jnp.float32),
            pltpu.VMEM((heads, 8, key_width), jnp.float32),
            pltpu.VMEM((heads, 8, 128), jnp.float32),
            pltpu.SemaphoreType.DMA((count,)),
            pltpu.SemaphoreType.DMA((count,)),
        ],
        compiler_params=pltpu.CompilerParams(
            collective_id=0, has_side_effects=True, vmem_limit_bytes=40 * 1024 * 1024
        ),
        cost_estimate=pl.CostEstimate(
            flops=30_000_000_000, bytes_accessed=8 * v.size, transcendentals=0
        ),
    )(state, q, k, v, gates, gain, lanes, cols)


def rows_kernel(pieces, x_ref, out_ref, own_sem, near_send, near_recv, far_send, far_recv, on_send, on_recv):
    me = lax.axis_index("tp")
    near = me + 1 - 2 * lax.rem(me, 2)
    far = lax.rem(me + 2, 4)
    opposite = lax.rem(near + 2, 4)
    size = x_ref.shape[0]
    step = size // pieces
    barrier = pltpu.get_barrier_semaphore()
    for other in (near, far):
        pl.semaphore_signal(barrier, inc=1, device_id={"tp": other}, device_id_type=MESH)
    pl.semaphore_wait(barrier, 2)

    def at(owner, p):
        return out_ref.at[pl.ds(pl.multiple_of(owner * size + p * step, step), step)]

    def send(src, dst, sems, p, target):
        return pltpu.make_async_remote_copy(
            src_ref=src,
            dst_ref=dst,
            send_sem=sems[0].at[p],
            recv_sem=sems[1].at[p],
            device_id={"tp": target},
            device_id_type=MESH,
        )

    mine = [x_ref.at[pl.ds(p * step, step)] for p in range(pieces)]
    far_out = [send(mine[p], at(me, p), (far_send, far_recv), p, far) for p in range(pieces)]
    near_out = [send(mine[p], at(me, p), (near_send, near_recv), p, near) for p in range(pieces)]
    far_in = [send(mine[p], at(far, p), (far_send, far_recv), p, far) for p in range(pieces)]
    near_in = [send(mine[p], at(near, p), (near_send, near_recv), p, near) for p in range(pieces)]
    onward = [send(at(far, p), at(far, p), (on_send, on_recv), p, near) for p in range(pieces)]
    on_in = [
        send(at(opposite, p), at(opposite, p), (on_send, on_recv), p, near)
        for p in range(pieces)
    ]
    for p in range(pieces):
        far_out[p].start()
    for p in range(pieces):
        near_out[p].start()
    whole = pl.ds(pl.multiple_of(me * size, size), size)
    own = pltpu.make_async_copy(x_ref, out_ref.at[whole], own_sem)
    own.start()
    for p in range(pieces):
        far_in[p].wait_recv()
        onward[p].start()
    own.wait()
    for p in range(pieces):
        near_in[p].wait_recv()
        on_in[p].wait_recv()
    for p in range(pieces):
        far_out[p].wait_send()
        near_out[p].wait_send()
        onward[p].wait_send()


def gather_rows(x):
    if lax.axis_size("tp") != 4:
        return lax.all_gather(x, "tp", axis=0, tiled=True)
    pieces = 4
    vmem = pl.BlockSpec(memory_space=pltpu.VMEM)
    return pl.pallas_call(
        functools.partial(rows_kernel, pieces),
        out_shape=jax.ShapeDtypeStruct((4 * x.shape[0], x.shape[1]), x.dtype),
        in_specs=[vmem],
        out_specs=vmem,
        scratch_shapes=[pltpu.SemaphoreType.DMA] + [pltpu.SemaphoreType.DMA((pieces,))] * 6,
        compiler_params=pltpu.CompilerParams(
            collective_id=1, has_side_effects=True, vmem_limit_bytes=16 * 1024 * 1024
        ),
        cost_estimate=pl.CostEstimate(
            flops=30_000_000_000, bytes_accessed=4 * x.size, transcendentals=0
        ),
    )(x)


def product_kernel(
    pieces,
    x_ref,
    w_ref,
    out_ref,
    pair_out,
    pair_in,
    far_out,
    far_in,
    near_out,
    near_in,
    pair_send,
    pair_recv,
    far_send,
    far_recv,
    near_send,
    near_recv,
):
    me = lax.axis_index("tp")
    near = me + 1 - 2 * lax.rem(me, 2)
    far = lax.rem(me + 2, 4)
    opposite = lax.rem(near + 2, 4)
    size = out_ref.shape[0]
    step = out_ref.shape[1] // pieces
    barrier = pltpu.get_barrier_semaphore()
    for other in (near, far):
        pl.semaphore_signal(barrier, inc=1, device_id={"tp": other}, device_id_type=MESH)
    pl.semaphore_wait(barrier, 2)

    def columns(p):
        return pl.ds(pl.multiple_of(p * step, step), step)

    def term(owner, p):
        rows = pl.ds(pl.multiple_of(owner * size, size), size)
        return jnp.dot(x_ref[rows, :], w_ref[:, columns(p)], preferred_element_type=jnp.float32)

    def send(src, dst, sems, p, target):
        return pltpu.make_async_remote_copy(
            src_ref=src.at[p],
            dst_ref=dst.at[p],
            send_sem=sems[0].at[p],
            recv_sem=sems[1].at[p],
            device_id={"tp": target},
            device_id_type=MESH,
        )

    def pair(p):
        return send(pair_out, pair_in, (pair_send, pair_recv), p, near)

    def across(p):
        return send(far_out, far_in, (far_send, far_recv), p, far)

    def beside(p):
        return send(near_out, near_in, (near_send, near_recv), p, near)

    @pl.loop(0, pieces)
    def _(p):
        pair_out[p] = term(opposite, p).astype(jnp.bfloat16)
        pair(p).start()
        mine = term(far, p)
        pair(p).wait_recv()
        far_out[p] = (mine + pair_in[p].astype(jnp.float32)).astype(jnp.bfloat16)
        across(p).start()

    @pl.loop(0, pieces)
    def _(p):
        near_out[p] = term(near, p).astype(jnp.bfloat16)
        beside(p).start()

    @pl.loop(0, pieces)
    def _(p):
        own = term(me, p)
        beside(p).wait_recv()
        out_ref[:, columns(p)] = own + near_in[p].astype(jnp.float32)

    @pl.loop(0, pieces)
    def _(p):
        across(p).wait_recv()
        out_ref[:, columns(p)] += far_in[p].astype(jnp.float32)

    @pl.loop(0, pieces)
    def _(p):
        pair(p).wait_send()
        across(p).wait_send()
        beside(p).wait_send()


def product_rows(x, w, tag):
    if lax.axis_size("tp") != 4:
        partial = jnp.dot(x, w, preferred_element_type=jnp.float32).astype(jnp.bfloat16)
        return lax.psum_scatter(partial, "tp", scatter_dimension=0, tiled=True).astype(
            jnp.float32
        )
    pieces = 4
    rows, wide = x.shape[0] // 4, w.shape[1]
    vmem = pl.BlockSpec(memory_space=pltpu.VMEM)
    slots = pltpu.VMEM((pieces, rows, wide // pieces), jnp.bfloat16)
    return pl.pallas_call(
        functools.partial(product_kernel, pieces),
        out_shape=jax.ShapeDtypeStruct((rows, wide), jnp.float32),
        in_specs=[vmem] * 2,
        out_specs=vmem,
        scratch_shapes=[slots] * 6 + [pltpu.SemaphoreType.DMA((pieces,))] * 6,
        compiler_params=pltpu.CompilerParams(
            collective_id=tag, has_side_effects=True, vmem_limit_bytes=40 * 1024 * 1024
        ),
        cost_estimate=pl.CostEstimate(
            flops=30_000_000_000, bytes_accessed=2 * w.size, transcendentals=0
        ),
    )(x, w)


def walk_kernel(count, pieces, x_ref, out_ref, own_sem, send_sem, recv_sem):
    me = lax.axis_index("sp")
    odd = lax.rem(me, 2)
    place = me // 2 + odd * (count - 1 - 2 * (me // 2))
    size = x_ref.shape[0]
    step = size // (2 * pieces)

    def index(position):
        position = lax.rem(position + 2 * count, count)
        back = position // (count // 2)
        return (1 - back) * 2 * position + back * (2 * (count - 1 - position) + 1)

    ways = (1, -1)
    barrier = pltpu.get_barrier_semaphore()
    for way in ways:
        pl.semaphore_signal(
            barrier, inc=1, device_id={"sp": index(place + way)}, device_id_type=MESH
        )
    pl.semaphore_wait(barrier, 2)

    def hop(w, t, p, age, own=False):
        inner = (w * pieces + p) * step
        owner = index(place - ways[w] * age)
        dst = out_ref.at[pl.ds(pl.multiple_of(owner * size + inner, step), step)]
        return pltpu.make_async_remote_copy(
            src_ref=x_ref.at[pl.ds(inner, step)] if own else dst,
            dst_ref=dst,
            send_sem=send_sem.at[w, p, t],
            recv_sem=recv_sem.at[w, p, t],
            device_id={"sp": index(place + ways[w])},
            device_id_type=MESH,
        )

    for p in range(pieces):
        for w in range(2):
            hop(w, 0, p, 0, True).start()
    whole = pl.ds(pl.multiple_of(me * size, size), size)
    own = pltpu.make_async_copy(x_ref, out_ref.at[whole], own_sem)
    own.start()

    @pl.loop(1, count - 1)
    def _(t):
        for p in range(pieces):
            for w in range(2):
                hop(w, t - 1, p, t).wait_recv()
                hop(w, t, p, t).start()

    own.wait()
    for p in range(pieces):
        for w in range(2):
            hop(w, count - 2, p, count - 1).wait_recv()
            hop(w, 0, p, 0, True).wait_send()

    @pl.loop(1, count - 1)
    def _(t):
        for p in range(pieces):
            for w in range(2):
                hop(w, t, p, t).wait_send()


def walk_gather(x, pieces):
    count = lax.axis_size("sp")
    if count % 2 or count < 4 or x.shape[0] % (32 * pieces):
        return lax.all_gather(x, "sp", axis=0, tiled=True)
    vmem = pl.BlockSpec(memory_space=pltpu.VMEM)
    return pl.pallas_call(
        functools.partial(walk_kernel, count, pieces),
        out_shape=jax.ShapeDtypeStruct((count * x.shape[0], x.shape[1]), x.dtype),
        in_specs=[vmem],
        out_specs=vmem,
        scratch_shapes=[pltpu.SemaphoreType.DMA]
        + [pltpu.SemaphoreType.DMA((2, pieces, count - 1))] * 2,
        compiler_params=pltpu.CompilerParams(
            collective_id=4, has_side_effects=True, vmem_limit_bytes=16 * 1024 * 1024
        ),
        cost_estimate=pl.CostEstimate(
            flops=30_000_000_000, bytes_accessed=count * x.size, transcendentals=0
        ),
    )(x)


def local(
    residual_entry_input,
    query_matrix_rows,
    key_matrix_rows,
    value_matrix_rows,
    output_gate_logits,
    input_gate_logits,
    forget_gate_logits,
    forget_decay_offset,
    head_norm_gain,
    cell_output_weight,
    feedforward_norm_gain,
    gate_up_weight,
    value_up_weight,
    gate_filter_taps,
    value_filter_taps,
    down_projection_weight,
):
    input_log, forget_log = gate_log_values(
        input_gate_logits, forget_gate_logits, forget_decay_offset
    )
    whole_gate = lax.all_gather(gate_up_weight, "sp", axis=0, tiled=True)
    whole_down = lax.all_gather(down_projection_weight, "sp", axis=1, tiled=True)
    gated_rows = cell(
        query_matrix_rows,
        key_matrix_rows,
        value_matrix_rows,
        output_gate_logits,
        input_log,
        forget_log,
        head_norm_gain,
    )
    mixed_rows = product_rows(gated_rows, cell_output_weight, 2)
    stream_wide = residual_entry_input.astype(jnp.float32) + mixed_rows
    stream = stream_wide.astype(jnp.bfloat16)
    stream_wide = lax.optimization_barrier(stream).astype(jnp.float32)
    normed_rows = (
        stream_wide
        * lax.rsqrt(jnp.mean(stream_wide * stream_wide, axis=-1, keepdims=True) + eps)
        * feedforward_norm_gain[None, :]
    ).astype(jnp.bfloat16)
    group_rows = gather_rows(normed_rows)
    group_rows, value_shard = lax.optimization_barrier((group_rows, value_up_weight))
    whole_value = walk_gather(value_shard, 2)
    earlier_rows = shifted(group_rows[-2:], "sp", 1)
    window = jnp.concatenate([earlier_rows, group_rows], axis=0)
    up_gate = jnp.dot(
        window,
        whole_gate,
        preferred_element_type=jnp.float32,
    )
    up_value = jnp.dot(
        window,
        whole_value,
        preferred_element_type=jnp.float32,
    )
    conv_g = (
        gate_filter_taps[0][None, :] * up_gate[:-2]
        + gate_filter_taps[1][None, :] * up_gate[1:-1]
        + gate_filter_taps[2][None, :] * up_gate[2:]
    )
    conv_v = (
        value_filter_taps[0][None, :] * up_value[:-2]
        + value_filter_taps[1][None, :] * up_value[1:-1]
        + value_filter_taps[2][None, :] * up_value[2:]
    )
    hidden = (jax.nn.silu(conv_g) * conv_v).astype(jnp.bfloat16)
    ffn_rows = product_rows(hidden, whole_down, 3)
    return (stream_wide + ffn_rows).astype(jnp.bfloat16)


def solution(mesh):
    in_specs = (
        P(("sp", "tp"), None),
        P("sp", "tp"),
        P("sp", "tp"),
        P("sp", "tp"),
        P("sp", "tp"),
        P("sp", "tp"),
        P("sp", "tp"),
        P("sp", "tp"),
        P("tp", None),
        P("tp", None),
        P(),
        P("sp", "tp"),
        P("sp", "tp"),
        P(None, "tp"),
        P(None, "tp"),
        P("tp", "sp"),
    )
    out_specs = P(("sp", "tp"), None)
    return jax.shard_map(local, mesh=mesh, in_specs=in_specs, out_specs=out_specs, check_vma=False)
```

profile of v0, /device:TPU:29, one launch (start us, length us, event | category | flops | bytes accessed | tf_op | source)
XLA Modules:
  0.0 323.2 jit_solution(9407974556567575655)
XLA Ops:
  6.5 0.0 all-gather.3.cloned.1.call-start
  6.6 0.7 all-gather.3.cloned.1.call-update
  7.3 0.0 all-gather.5.cloned.1.call-start
  7.3 0.7 all-gather.5.cloned.1.call-update
  8.0 0.7 fusion.22
  8.8 0.2 fusion.15
  8.9 0.1 copy.61
  9.0 0.2 slice_reduce_fusion.6
  9.2 0.1 copy.36
  9.3 0.1 convolution_add_fusion
  9.4 0.1 copy.37
  9.5 0.9 add_reduce_fusion
  10.4 0.1 fusion.25
  10.5 1.1 mul.107
  11.6 2.5 copy.46
  14.2 2.2 copy.45
  16.4 1.4 multiply_reduce_fusion
  17.8 0.1 copy.43
  17.9 0.2 copy.44
  18.2 1.6 convolution_convert_fusion
  19.8 0.1 broadcast_in_dim.68
  19.9 0.1 broadcast_in_dim.65
  20.0 0.1 broadcast_in_dim.66
  20.0 0.1 broadcast_in_dim.63
  20.1 0.1 broadcast_in_dim.64
  20.2 0.2 concatenate.12
  20.4 0.0 copy-start.7
  20.4 1.1 copy-done.7
  21.5 57.3 %shard_map.154.x_ref = bf16[1024,512]{1,0:T(8,128)(2,1)S(1)} custom-call(bf16[288,256]{1,0:T(8,128)(2,1)S(1)} %bitcast.46, bf16[1024,256]{1,0:T(8,128)(2,1)S(1)} %copy-done.7, bf16[1024,256]{1,0:T(8,128)(2,1)S(1)} %copy-done, bf16[1024,512]{1,0:T(8,128)(2,1)S(1)} %copy-done.1, bf16[1024,512]{1,0:T(8,128)(2,1)S(1)} %copy-done.5, f32[2,256]{1,0:T(2,128)S(1)} %copy-done.8, ...), custom_call_target="tpu_custom_call" | custom-call | flops 30000001024 | bytes 4194304 | tf_op jit(solution)/shard_map/pallas_call | solution.py:228
  78.8 0.0 copy-start.12
  78.8 0.0 copy-start.15
  78.8 27.8 %shard_map.155 = f32[256,2048]{1,0:T(8,128)S(1)} custom-call(bf16[1024,512]{1,0:T(8,128)(2,1)S(1)} %shard_map.154.x_ref, bf16[512,2048]{1,0:T(8,128)(2,1)S(1)} %copy-done.4), custom_call_target="tpu_custom_call" | custom-call | flops 30000001024 | bytes 2097152 | tf_op jit(solution)/shard_map/pallas_call | solution.py:422
  106.6 0.3 add_convert_fusion
  106.9 0.0 copy-start.10
  106.9 0.3 fusion.8
  107.2 0.3 fusion.10.x_ref
  107.5 0.0 copy-start.6
  107.5 26.9 %shard_map.156 = bf16[1024,2048]{1,0:T(8,128)(2,1)S(1)} custom-call(bf16[256,2048]{1,0:T(8,128)(2,1)S(1)} %fusion.10.x_ref), custom_call_target="tpu_custom_call" | custom-call | flops 30000001024 | bytes 2097152 | tf_op jit(solution)/shard_map/pallas_call | solution.py:310
  134.5 1.6 collective-permute-start
  136.1 116.7 %shard_map.157 = bf16[2048,1408]{1,0:T(8,128)(2,1)S(1)} custom-call(bf16[256,1408]{1,0:T(8,128)(2,1)S(1)} %copy-done.6), custom_call_target="tpu_custom_call" | custom-call | flops 30000001024 | bytes 2883584 | tf_op jit(solution)/shard_map/pallas_call | solution.py:502
  252.8 0.1 slice_reduce_fusion.2
  253.0 8.7 %fusion.6 = f32[1026,1408]{1,0:T(8,128)} fusion(bf16[2048,1408]{1,0:T(8,128)(2,1)S(1)} %shard_map.157, bf16[1024,2048]{1,0:T(8,128)(2,1)S(1)} %shard_map.156, bf16[2,2048]{1,0:T(2,128)(2,1)S(1)} %collective-permute-done), kind=kOutput, calls=%fused_computation.16 | convolution fusion | flops 5925519360 | bytes 15748096 | tf_op jit(solution)/shard_map/dot_general | solution.py:569
  261.7 10.7 %fusion.7 = f32[1026,1408]{1,0:T(8,128)S(1)} fusion(bf16[2048,1408]{1,0:T(8,128)(2,1)} %all-gather.3.cloned.1.call-done, bf16[1024,2048]{1,0:T(8,128)(2,1)} %copy-done.2, bf16[2,2048]{1,0:T(2,128)(2,1)S(1)} %collective-permute-done), kind=kOutput, calls=%fused_computation.17 | convolution fusion | flops 5925519360 | bytes 15748096 | tf_op jit(solution)/shard_map/dot_general | solution.py:564
  272.4 4.7 %fusion.2.x_ref = bf16[1024,1408]{1,0:T(8,128)(2,1)S(1)} fusion(f32[1026,1408]{1,0:T(8,128)S(1)} %copy-done.9, f32[1026,1408]{1,0:T(8,128)S(1)} %fusion.7, f32[1408]{0:T(1024)S(1)} %get-tuple-element.13, f32[1408]{0:T(1024)S(1)} %get-tuple-element.14, f32[1408]{0:T(1024)S(1)} %get-tuple-element.12, f32[1408]{0:T(1024)S(1)} %get-tuple-element.28, ...), kind=kLoop, calls=%fused_computation.3 | loop fusion | flops 23068672 | bytes 37520384 | tf_op jit(solution)/shard_map/convert_element_type | solution.py:584
  277.1 0.0 all-gather.5.cloned.1.call-done.w_ref
  277.1 2.6 copy-done.3
  279.8 35.3 %shard_map.158 = f32[256,2048]{1,0:T(8,128)S(1)} custom-call(bf16[1024,1408]{1,0:T(8,128)(2,1)S(1)} %fusion.2.x_ref, bf16[1408,2048]{1,0:T(8,128)(2,1)S(1)} %copy-done.3), custom_call_target="tpu_custom_call" | custom-call | flops 30000001024 | bytes 5767168 | tf_op jit(solution)/shard_map/pallas_call | solution.py:422
  315.1 1.3 fusion.11
  (38 shorter events, 0.2 us)
Async XLA Ops:
  6.5 9.9 %copy-start = (bf16[1024,256]{1,0:T(8,128)(2,1)S(1)}, bf16[1024,256]{1,0:T(8,128)(2,1)}, u32[]{:S(2)}) copy-start(bf16[1024,256]{1,0:T(8,128)(2,1)} %k_ref.1) | copy-start | bytes 1572868
  6.5 11.6 %copy-start.1 = (bf16[1024,512]{1,0:T(8,128)(2,1)S(1)}, bf16[1024,512]{1,0:T(8,128)(2,1)}, u32[]{:S(2)}) copy-start(bf16[1024,512]{1,0:T(8,128)(2,1)} %v_ref.1) | copy-start | bytes 3145732
  6.5 13.8 %copy-start.5 = (bf16[1024,512]{1,0:T(8,128)(2,1)S(1)}, bf16[1024,512]{1,0:T(8,128)(2,1)}, u32[]{:S(2)}) copy-start(bf16[1024,512]{1,0:T(8,128)(2,1)} %gate_ref.1) | copy-start | bytes 3145732
  6.5 13.9 %copy-start.8 = (f32[2,256]{1,0:T(2,128)S(1)}, f32[2,256]{1,0:T(2,128)}, u32[]{:S(2)}) copy-start(f32[2,256]{1,0:T(2,128)} %gain_ref.1) | copy-start | bytes 6148
  6.5 255.1 %all-gather.3.cloned.1.call-start = ((), (), s32[]{:S(2)}) async-start(), calls=%async_computation | async-start | bytes 6488064 | tf_op jit(solution)/shard_map/all_gather | solution.py:539
  7.3 269.8 %all-gather.5.cloned.1.call-start = ((), (), s32[]{:S(2)}) async-start(), calls=%async_computation.1 | async-start | bytes 6488064 | tf_op jit(solution)/shard_map/all_gather | solution.py:540
  20.4 1.1 copy-start.7
  21.5 57.3 %copy-start.4 = (bf16[512,2048]{1,0:T(8,128)(2,1)S(1)}, bf16[512,2048]{1,0:T(8,128)(2,1)}, u32[]{:S(2)}) copy-start(bf16[512,2048]{1,0:T(8,128)(2,1)} %w_ref.1) | copy-start | bytes 6291460
  78.8 27.8 %copy-start.12 = (bf16[256,2048]{1,0:T(8,128)(2,1)S(1)}, bf16[256,2048]{1,0:T(8,128)(2,1)}, u32[]{:S(2)}) copy-start(bf16[256,2048]{1,0:T(8,128)(2,1)} %param.16) | copy-start | bytes 3145732
  78.8 28.4 %copy-start.15 = (f32[2048]{0:T(1024)S(1)}, f32[2048]{0:T(1024)}, u32[]{:S(2)}) copy-start(f32[2048]{0:T(1024)} %param.26) | copy-start | bytes 24580
  106.9 27.5 %copy-start.10 = (bf16[256,2048]{1,0:T(8,128)(2,1)}, bf16[256,2048]{1,0:T(8,128)(2,1)S(1)}, u32[]{:S(2)}) copy-start(bf16[256,2048]{1,0:T(8,128)(2,1)S(1)} %add_convert_fusion) | copy-start | bytes 3145732
  107.5 28.6 %copy-start.6 = (bf16[256,1408]{1,0:T(8,128)(2,1)S(1)}, bf16[256,1408]{1,0:T(8,128)(2,1)}, u32[]{:S(2)}) copy-start(bf16[256,1408]{1,0:T(8,128)(2,1)} %x_ref) | copy-start | bytes 2162692
  134.4 118.5 %copy-start.2 = (bf16[1024,2048]{1,0:T(8,128)(2,1)}, bf16[1024,2048]{1,0:T(8,128)(2,1)S(1)}, u32[]{:S(2)}) copy-start(bf16[1024,2048]{1,0:T(8,128)(2,1)S(1)} %shard_map.156) | copy-start | bytes 12582916
  134.4 118.4 %copy-start.13 = (f32[3,1408]{1,0:T(4,128)S(1)}, f32[3,1408]{1,0:T(4,128)}, u32[]{:S(2)}) copy-start(f32[3,1408]{1,0:T(4,128)} %param.30) | copy-start | bytes 50692
  134.4 118.4 %copy-start.14 = (f32[3,1408]{1,0:T(4,128)S(1)}, f32[3,1408]{1,0:T(4,128)}, u32[]{:S(2)}) copy-start(f32[3,1408]{1,0:T(4,128)} %param.29) | copy-start | bytes 50692
  134.5 118.5 %collective-permute-start = (bf16[2,2048]{1,0:T(2,128)(2,1)S(1)}, bf16[2,2048]{1,0:T(2,128)(2,1)S(1)}, u32[]{:S(2)}, u32[]{:S(2)}) collective-permute-start(bf16[2,2048]{1,0:T(2,128)(2,1)S(1)} %slice.44), channel_id=1, source_target_pairs={{0,4},{4,8},{8,12},{12,16},{16,20},{20,24},{24,28},{1,5},{5,9},{9,... | collective-permute-start | bytes 24584 | tf_op jit(solution)/shard_map/ppermute | solution.py:20
  261.7 10.7 %copy-start.9 = (f32[1026,1408]{1,0:T(8,128)S(1)}, f32[1026,1408]{1,0:T(8,128)}, u32[]{:S(2)}) copy-start(f32[1026,1408]{1,0:T(8,128)} %fusion.6) | copy-start | bytes 17335300
  277.1 2.6 copy-start.3
  279.8 35.3 %copy-start.11 = (bf16[256,2048]{1,0:T(8,128)(2,1)S(1)}, bf16[256,2048]{1,0:T(8,128)(2,1)}, u32[]{:S(2)}) copy-start(bf16[256,2048]{1,0:T(8,128)(2,1)} %copy-done.10) | copy-start | bytes 3145732
Sparse Core Ops, SparseCore 0:
  9.5 112.5 all-gather.2
  124.2 135.3 all-gather.4
where the time goes:
time: 324 us; the launch traced here: 323 us
  Pallas kernels  264 us (81%)
  matrix products  21.4 us (7%)
  between operations  13.8 us (4%)
  local copies, waits for them, and re-layouts  10.8 us (3%)
  other arithmetic  10.2 us (3%)
    pallas_call x1, Pallas kernels, walk_gather(): pl.pallas_call(functools.partial(walk_kernel, count, pieces), out_shape=j...  117 us
    pallas_call x2, Pallas kernels, product_rows(): pl.pallas_call(functools.partial(product_kernel, pieces), out_shape=jax.S...  63.1 us
    pallas_call x1, Pallas kernels, cell(): pl.pallas_call(functools.partial(cell_kernel, count, heads), out_shape=ja...  57.3 us
    pallas_call x1, Pallas kernels, gather_rows(): pl.pallas_call(functools.partial(rows_kernel, pieces), out_shape=jax.Shap...  26.9 us
    dot_general x1, matrix products, local(): up_gate = jnp.dot(window, whole_gate, preferred_element_type=jnp.float32)  10.7 us
    dot_general x1, matrix products, local(): up_value = jnp.dot(window, whole_value, preferred_element_type=jnp.float32)  8.72 us
  transfers between devices with their start and end apart: 3, of which 0 were waited for; matrix products, arithmetic and copies ran while one was open for 12% of the time, Pallas kernels for 71%

commit v1 on v0

--- a/solution.py
+++ b/solution.py
@@ -179,7 +179,7 @@
     return (high.astype(jnp.bfloat16), (x - high).astype(jnp.bfloat16))
 
 
-def cell(q, k, v, gates, input_log, forget_log, gain):
+def cell_parts(q, k, v, input_log, forget_log):
     heads = input_log.shape[1]
     tokens = q.shape[0]
     key_width = q.shape[1] // heads
@@ -224,6 +224,16 @@
         axis=1,
     )
     cols = jnp.concatenate([within, shifted_log], axis=2).reshape(tokens, 2 * heads)
+    return state, lanes, cols
+
+
+def cell(q, k, v, gates, input_log, forget_log, gain):
+    heads = input_log.shape[1]
+    key_width = q.shape[1] // heads
+    value_width = v.shape[1] // heads
+    count = lax.axis_size("sp")
+    span = key_width + STATE_PAD
+    state, lanes, cols = cell_parts(q, k, v, input_log, forget_log)
     vmem = pl.BlockSpec(memory_space=pltpu.VMEM)
     return pl.pallas_call(
         functools.partial(cell_kernel, count, heads),
@@ -515,6 +525,749 @@
     )(x)
 
 
+def layer_kernel(
+    count,
+    heads,
+    up_pieces,
+    down_pieces,
+    logs_ref,
+    q_ref,
+    k_ref,
+    v_ref,
+    gate_ref,
+    gain_ref,
+    wo_ref,
+    residual_ref,
+    norm_gain_ref,
+    gate_taps_ref,
+    value_taps_ref,
+    gate_w_ref,
+    value_w_ref,
+    down_w_ref,
+    out_ref,
+    rows_ref,
+    cols_ref,
+    state_ref,
+    held,
+    memory,
+    normer,
+    running,
+    pair_memory,
+    pair_normer,
+    pair_level,
+    handed,
+    gated,
+    pair_out,
+    pair_in,
+    far_out,
+    far_in,
+    near_out,
+    near_in,
+    total_rows,
+    stream,
+    group,
+    full_up,
+    full_down,
+    up_tile,
+    hidden,
+    load_sem,
+    state_send,
+    state_recv,
+    up_send,
+    up_recv,
+    down_send,
+    down_recv,
+    first_sem,
+    second_sem,
+    rows_sem,
+    edge_sem,
+):
+    me = lax.axis_index("sp")
+    tp = lax.axis_index("tp")
+    near = tp + 1 - 2 * lax.rem(tp, 2)
+    far = lax.rem(tp + 2, 4)
+    opposite = lax.rem(near + 2, 4)
+    odd = lax.rem(me, 2)
+    half = count // 2
+    place = me // 2 + odd * (count - 1 - 2 * (me // 2))
+    tiles = full_up.shape[0]
+    up_rows = full_up.shape[1] // count
+    up_step = up_rows // (2 * up_pieces)
+    down_step = full_down.shape[1] // (2 * down_pieces)
+    lane = full_up.shape[2] // 2
+
+    barrier = pltpu.get_barrier_semaphore()
+    for d in range(1, count):
+        pl.semaphore_signal(
+            barrier, inc=1, device_id={"sp": lax.rem(me + d, count)}, device_id_type=MESH
+        )
+    for other in (near, far):
+        pl.semaphore_signal(barrier, inc=1, device_id={"tp": other}, device_id_type=MESH)
+
+    own_up = pl.ds(pl.multiple_of(me * up_rows, up_rows), up_rows)
+    loads = []
+    for i in range(tiles):
+        for a, w_ref in enumerate((gate_w_ref, value_w_ref)):
+            loads.append(
+                pltpu.make_async_copy(
+                    w_ref.at[:, pl.ds(i * lane, lane)],
+                    full_up.at[i, own_up, pl.ds(a * lane, lane)],
+                    load_sem.at[2 * i + a],
+                )
+            )
+    down_load = pltpu.make_async_copy(down_w_ref, full_down.at[me], load_sem.at[2 * tiles])
+    for load in loads:
+        load.start()
+    down_load.start()
+
+    pl.semaphore_wait(barrier, count + 1)
+
+    step_at = me // 2
+    swap = pltpu.make_async_remote_copy(
+        src_ref=state_ref,
+        dst_ref=held.at[0],
+        send_sem=state_send.at[0],
+        recv_sem=state_recv.at[0],
+        device_id={"sp": me + 1 - 2 * odd},
+        device_id_type=MESH,
+    )
+    hand = pltpu.make_async_remote_copy(
+        src_ref=handed,
+        dst_ref=held.at[1],
+        send_sem=state_send.at[1],
+        recv_sem=state_recv.at[1],
+        device_id={"sp": lax.rem(me + 2, count)},
+        device_id_type=MESH,
+    )
+    def index(position):
+        position = lax.rem(position + 2 * count, count)
+        back = position // half
+        return (1 - back) * 2 * position + back * (2 * (count - 1 - position) + 1)
+
+    ways = (1, -1)
+
+    def up_hop(w, t, m):
+        owner = index(place - ways[w] * t)
+        row = owner * up_rows + (w * up_pieces + m) * up_step
+        part = full_up.at[:, pl.ds(pl.multiple_of(row, up_step), up_step), :]
+        return pltpu.make_async_remote_copy(
+            src_ref=part,
+            dst_ref=part,
+            send_sem=up_send.at[w, m, t],
+            recv_sem=up_recv.at[w, m, t],
+            device_id={"sp": index(place + ways[w])},
+            device_id_type=MESH,
+        )
+
+    def down_hop(w, t, m):
+        owner = index(place - ways[w] * t)
+        row = (w * down_pieces + m) * down_step
+        part = full_down.at[owner, pl.ds(pl.multiple_of(row, down_step), down_step), :]
+        return pltpu.make_async_remote_copy(
+            src_ref=part,
+            dst_ref=part,
+            send_sem=down_send.at[w, m, t],
+            recv_sem=down_recv.at[w, m, t],
+            device_id={"sp": index(place + ways[w])},
+            device_id_type=MESH,
+        )
+
+    up_ticks = (count - 1) * up_pieces
+    all_ticks = up_ticks + (count - 1) * down_pieces
+
+    def move(hop, pieces, n):
+        t = n // pieces
+        m = lax.rem(n, pieces)
+        for w in range(2):
+
+            @pl.when(t > 0)
+            def _():
+                hop(w, t - 1, m).wait_recv()
+
+            hop(w, t, m).start()
+
+    def up_tick(n):
+        move(up_hop, up_pieces, n)
+
+    def tick(n):
+        @pl.when(n < up_ticks)
+        def _():
+            up_tick(n)
+
+        @pl.when((n >= up_ticks) & (n < all_ticks))
+        def _():
+            move(down_hop, down_pieces, n - up_ticks)
+
+    def up_sent(n):
+        for w in range(2):
+            up_hop(w, n // up_pieces, lax.rem(n, up_pieces)).wait_send()
+
+    for load in loads:
+        load.wait()
+    down_load.wait()
+    for n in range(2):
+        up_tick(n)
+
+    key_width = memory.shape[1]
+    value_width = memory.shape[2]
+    span = key_width + STATE_PAD
+
+    def read_state(ref, h):
+        low = h * span
+        extra = ref[low + key_width : low + span, :].astype(jnp.float32)
+        total = extra[2:3, :1] + extra[3:4, :1]
+        level = extra[4:5, :1] + extra[5:6, :1]
+        parts = extra[0:1, :key_width] + extra[1:2, :key_width]
+        return ref[low : low + key_width, :].astype(jnp.float32), parts, level, total
+
+    def join(first, second, total):
+        mem_a, norm_a, level_a = first
+        mem_b, norm_b, level_b = second
+        after = jnp.maximum(total + level_a, level_b)
+        one = jnp.exp(total + level_a - after)
+        two = jnp.exp(level_b - after)
+        return one * mem_a + two * mem_b, one * norm_a + two * norm_b, after
+
+    def keep(refs, h, values):
+        mem, norm, level = values
+        refs[0][h] = mem
+        refs[1][h, :1, :] = norm
+        refs[2][h] = jnp.broadcast_to(level, refs[2].shape[1:])
+
+    carried_refs = (memory, normer, running)
+
+    def write_state(ref, h, mem, norm, level, total):
+        low = h * span
+        ref[low : low + key_width, :] = mem.astype(jnp.bfloat16)
+        lines = jnp.zeros((STATE_PAD, value_width), jnp.float32)
+        at_line = lax.broadcasted_iota(jnp.int32, lines.shape, 0)
+        norm = jnp.concatenate([norm] * (value_width // key_width), axis=1)
+        for i, part in enumerate((norm, total, level)):
+            high = part.astype(jnp.bfloat16).astype(jnp.float32)
+            lines = jnp.where(at_line == 2 * i, high, lines)
+            lines = jnp.where(at_line == 2 * i + 1, part - high, lines)
+        ref[low + key_width : low + span, :] = lines.astype(jnp.bfloat16)
+
+    length = BLOCK
+    blocks = q_ref.shape[0] // length
+    at_row = lax.broadcasted_iota(jnp.int32, (length, length), 0)
+    at_col = lax.broadcasted_iota(jnp.int32, (length, length), 1)
+
+    def by_block(first):
+        return jnp.concatenate(
+            [
+                logs_ref[first : first + heads, b * length : (b + 1) * length]
+                for b in range(blocks)
+            ],
+            axis=0,
+        )
+
+    within = jnp.dot(
+        by_block(heads),
+        jnp.where(at_row <= at_col, 1.0, 0.0),
+        precision=lax.Precision.HIGHEST,
+        preferred_element_type=jnp.float32,
+    )
+    shifted_all = by_block(0) - within
+    each_all = within[:, length - 1 : length]
+    after = jnp.zeros((heads, 1), jnp.float32)
+    to_end = [None] * blocks
+    for b in reversed(range(blocks)):
+        part = slice(b * heads, (b + 1) * heads)
+        after = after + each_all[part]
+        to_end[b] = shifted_all[part] + after
+    own_total = after
+    own_level = functools.reduce(jnp.maximum, to_end)
+    own_level = jnp.max(own_level, axis=1, keepdims=True)
+    for b in range(blocks):
+        part = slice(b * heads, (b + 1) * heads)
+        rows_ref[b, 0 : 2 * heads, :] = jnp.concatenate(
+            [shifted_all[part], jnp.broadcast_to(each_all[part], (heads, length))], axis=0
+        )
+        lines = [within[part], shifted_all[part], jnp.exp(to_end[b] - own_level)]
+        lines.append(jnp.zeros((length - 3 * heads, length), jnp.float32))
+        cols_ref[b * length : (b + 1) * length, :] = jnp.transpose(
+            jnp.concatenate(lines, axis=0)
+        )
+
+    memory[...] = jnp.zeros_like(memory)
+    normer[...] = jnp.zeros_like(normer)
+
+    @pl.loop(0, blocks)
+    def _(j):
+        rows = pl.ds(pl.multiple_of(j * length, length), length)
+        cols = cols_ref[rows, :]
+        for h in range(heads):
+            k = k_ref[rows, h * key_width : (h + 1) * key_width]
+            v = v_ref[rows, h * value_width : (h + 1) * value_width]
+            weighted = k.astype(jnp.float32) * cols[:, 2 * heads + h : 2 * heads + h + 1]
+            memory[h] += lax.dot_general(
+                weighted.astype(jnp.bfloat16),
+                v,
+                (((0,), (0,)), ((), ())),
+                preferred_element_type=jnp.float32,
+            )
+            normer[h, :1, :] += jnp.sum(weighted, axis=0, keepdims=True)
+
+    for h in range(heads):
+        write_state(
+            state_ref,
+            h,
+            memory[h],
+            normer[h, :1, :],
+            own_level[h : h + 1, :],
+            own_total[h : h + 1, :],
+        )
+    swap.start()
+    swap.wait_recv()
+
+    @pl.when(odd == 0)
+    def _():
+        for h in range(heads):
+            mem_a, norm_a, level_a, total_a = read_state(state_ref, h)
+            mem_b, norm_b, level_b, total_b = read_state(held.at[0], h)
+            out = join((mem_a, norm_a, level_a), (mem_b, norm_b, level_b), total_b)
+            keep((pair_memory, pair_normer, pair_level.at[0]), h, out)
+            pair_level[1, h] = jnp.broadcast_to(total_a + total_b, pair_level.shape[2:])
+
+    @pl.when(odd == 1)
+    def _():
+        for h in range(heads):
+            mem_a, norm_a, level_a, total_a = read_state(held.at[0], h)
+            mem_b, norm_b, level_b, total_b = read_state(state_ref, h)
+            out = join((mem_a, norm_a, level_a), (mem_b, norm_b, level_b), total_b)
+            keep((pair_memory, pair_normer, pair_level.at[0]), h, out)
+            pair_level[1, h] = jnp.broadcast_to(total_a + total_b, pair_level.shape[2:])
+
+    started = jnp.minimum(FIRST_TICKS + NEXT_TICKS * step_at, up_ticks)
+
+    @pl.loop(2, started)
+    def _(n):
+        up_sent(n - 2)
+        up_tick(n)
+
+    memory[...] = jnp.zeros_like(memory)
+    normer[...] = jnp.zeros_like(normer)
+    running[...] = jnp.full(running.shape, neg_large, jnp.float32)
+
+    @pl.when(step_at > 0)
+    def _():
+        hand.wait_recv()
+        for h in range(heads):
+            mem, parts, level, total = read_state(held.at[1], h)
+            keep(carried_refs, h, (mem, parts, level))
+
+    @pl.when(step_at + 1 < half)
+    def _():
+        for h in range(heads):
+            mem, norm, level = join(
+                (memory[h], normer[h, :1, :], running[h, :1, :1]),
+                (pair_memory[h], pair_normer[h, :1, :], pair_level[0, h, :1, :1]),
+                pair_level[1, h, :1, :1],
+            )
+            write_state(handed, h, mem, norm, level, jnp.zeros_like(level))
+        hand.start()
+
+    @pl.when(odd == 1)
+    def _():
+        for h in range(heads):
+            mem, norm, level, total = read_state(held.at[0], h)
+            out = join(
+                (memory[h], normer[h, :1, :], running[h, :1, :1]), (mem, norm, level), total
+            )
+            keep(carried_refs, h, out)
+
+    scale = key_width ** (-0.5)
+    causal = at_col <= at_row
+
+    @pl.loop(0, blocks)
+    def _(j):
+        tick(started + j)
+        rows = pl.ds(pl.multiple_of(j * length, length), length)
+        lanes = rows_ref[j]
+        cols = cols_ref[rows, :]
+        for h in range(heads):
+            keys = slice(h * key_width, (h + 1) * key_width)
+            vals = slice(h * value_width, (h + 1) * value_width)
+            q = q_ref[rows, keys]
+            k = k_ref[rows, keys]
+            v = v_ref[rows, vals]
+            before = running[h, :1, :1]
+            total = lanes[heads + h : heads + h + 1, :1]
+            shifted_log = jnp.where(causal, lanes[h : h + 1, :], -jnp.inf)
+            top = jnp.maximum(jnp.max(shifted_log, axis=1, keepdims=True), before)
+            raw = (
+                lax.dot_general(
+                    q, k, (((1,), (1,)), ((), ())), preferred_element_type=jnp.float32
+                )
+                * scale
+            )
+            scores = raw * jnp.exp(shifted_log - top)
+            carry = jnp.exp(before - top) * scale
+            state = memory[h]
+            high = state.astype(jnp.bfloat16)
+            low = (state - high.astype(jnp.float32)).astype(jnp.bfloat16)
+            carried = jnp.dot(q, high, preferred_element_type=jnp.float32) + jnp.dot(
+                q, low, preferred_element_type=jnp.float32
+            )
+            numerator = carry * carried + jnp.dot(
+                scores.astype(jnp.bfloat16), v, preferred_element_type=jnp.float32
+            )
+            denominator = carry * jnp.sum(
+                q.astype(jnp.float32) * normer[h, :1, :], axis=1, keepdims=True
+            ) + jnp.sum(scores, axis=1, keepdims=True)
+            level = cols[:, h : h + 1] + top
+            value = numerator / jnp.maximum(jnp.abs(denominator), jnp.exp(-level))
+            mean = jnp.mean(value * value, axis=1, keepdims=True)
+            normed = value * lax.rsqrt(mean + eps) * gain_ref[h : h + 1, :]
+            gate = normed * jax.nn.sigmoid(gate_ref[rows, vals].astype(jnp.float32))
+            gated[rows, vals] = gate.astype(gated.dtype)
+            last = jnp.max(jnp.maximum(lanes[h : h + 1, :], before), axis=1, keepdims=True)
+            decay = jnp.exp(before - last)
+            weighted = k.astype(jnp.float32) * jnp.exp(cols[:, heads + h : heads + h + 1] - last)
+            memory[h] = decay * state + lax.dot_general(
+                weighted.astype(jnp.bfloat16),
+                v,
+                (((0,), (0,)), ((), ())),
+                preferred_element_type=jnp.float32,
+            )
+            normer[h, :1, :] = decay * normer[h, :1, :] + jnp.sum(
+                weighted, axis=0, keepdims=True
+            )
+            running[h] = jnp.broadcast_to(last + total, running.shape[1:])
+
+    size = residual_ref.shape[0]
+    slices = pair_out.shape[0]
+    wide = pair_out.shape[2]
+
+    def columns(i):
+        return pl.ds(pl.multiple_of(i * wide, wide), wide)
+
+    def exchange(src, dst, sems, kind, i, target):
+        return pltpu.make_async_remote_copy(
+            src_ref=src.at[i],
+            dst_ref=dst.at[i],
+            send_sem=sems.at[2 * kind, i],
+            recv_sem=sems.at[2 * kind + 1, i],
+            device_id={"tp": target},
+            device_id_type=MESH,
+        )
+
+    def pair(sems, i):
+        return exchange(pair_out, pair_in, sems, 0, i, near)
+
+    def across(sems, i):
+        return exchange(far_out, far_in, sems, 1, i, far)
+
+    def beside(sems, i):
+        return exchange(near_out, near_in, sems, 2, i, near)
+
+    def product_slice(x_ref, weight, sems, i):
+        def term(owner):
+            rows = pl.ds(pl.multiple_of(owner * size, size), size)
+            return jnp.dot(x_ref[rows, :], weight(), preferred_element_type=jnp.float32)
+
+        pair_out[i] = term(opposite).astype(jnp.bfloat16)
+        pair(sems, i).start()
+        onward = term(far)
+        near_out[i] = term(near).astype(jnp.bfloat16)
+        beside(sems, i).start()
+        pair(sems, i).wait_recv()
+        far_out[i] = (onward + pair_in[i].astype(jnp.float32)).astype(jnp.bfloat16)
+        across(sems, i).start()
+        own = term(tp)
+        beside(sems, i).wait_recv()
+        return own + near_in[i].astype(jnp.float32)
+
+    @pl.loop(0, slices)
+    def _(i):
+        tick(started + blocks + i)
+        total_rows[:, columns(i)] = product_slice(
+            gated, lambda: wo_ref[:, columns(i)], first_sem, i
+        )
+
+    @pl.loop(0, slices)
+    def _(i):
+        across(first_sem, i).wait_recv()
+        total_rows[:, columns(i)] += far_in[i].astype(jnp.float32)
+
+    pad = group.shape[0] - 4 * size
+    row_pieces = rows_sem.shape[1]
+    row_step = size // row_pieces
+
+    def at(owner, p):
+        row = pad + owner * size + p * row_step
+        return group.at[pl.ds(pl.multiple_of(row, pad), row_step)]
+
+    def send_rows(owner, kind, p, target):
+        return pltpu.make_async_remote_copy(
+            src_ref=at(owner, p),
+            dst_ref=at(owner, p),
+            send_sem=rows_sem.at[2 * kind, p],
+            recv_sem=rows_sem.at[2 * kind + 1, p],
+            device_id={"tp": target},
+            device_id_type=MESH,
+        )
+
+    @pl.when(me == 0)
+    def _():
+        group[0:pad, :] = jnp.zeros((pad, group.shape[1]), group.dtype)
+
+    @pl.loop(0, row_pieces)
+    def _(p):
+        rows = pl.ds(pl.multiple_of(p * row_step, row_step), row_step)
+        rounded = (residual_ref[rows, :].astype(jnp.float32) + total_rows[rows, :]).astype(
+            jnp.bfloat16
+        )
+        stream[rows, :] = rounded
+        x = rounded.astype(jnp.float32)
+        normed = x * lax.rsqrt(jnp.mean(x * x, axis=-1, keepdims=True) + eps) * norm_gain_ref[...]
+        row = pad + tp * size + p * row_step
+        group[pl.ds(pl.multiple_of(row, pad), row_step), :] = normed.astype(jnp.bfloat16)
+        send_rows(tp, 0, p, far).start()
+        send_rows(tp, 1, p, near).start()
+
+    @pl.loop(0, row_pieces)
+    def _(p):
+        tick(started + blocks + slices + p)
+        send_rows(far, 0, p, far).wait_recv()
+        send_rows(far, 2, p, near).start()
+
+    @pl.loop(0, row_pieces)
+    def _(p):
+        send_rows(near, 1, p, near).wait_recv()
+        send_rows(opposite, 2, p, near).wait_recv()
+
+    edge = pltpu.make_async_remote_copy(
+        src_ref=group.at[pl.ds(4 * size, pad)],
+        dst_ref=group.at[pl.ds(0, pad)],
+        send_sem=edge_sem.at[0],
+        recv_sem=edge_sem.at[1],
+        device_id={"sp": lax.rem(me + 1, count)},
+        device_id_type=MESH,
+    )
+
+    @pl.when(me + 1 < count)
+    def _():
+        edge.start()
+
+    reached = jnp.maximum(started + blocks + slices + row_pieces, up_ticks)
+
+    @pl.loop(jnp.minimum(started + blocks + slices + row_pieces, up_ticks), up_ticks)
+    def _(n):
+        up_tick(n)
+
+    for m in range(up_pieces):
+        for w in range(2):
+            up_hop(w, count - 2, m).wait_recv()
+
+    @pl.when(me > 0)
+    def _():
+        edge.wait_recv()
+
+    @pl.loop(0, slices)
+    def _(i):
+        pair(first_sem, i).wait_send()
+        across(first_sem, i).wait_send()
+        beside(first_sem, i).wait_send()
+
+    early = up_ticks + half * down_pieces
+
+    @pl.loop(0, tiles)
+    def _(i):
+        @pl.when(reached + i < early)
+        def _():
+            tick(reached + i)
+
+        up_tile[...] = jnp.dot(group[...], full_up[i], preferred_element_type=jnp.float32)
+        tokens = 4 * size
+        at_lane = pl.ds(pl.multiple_of(i * lane, lane), lane)
+
+        def conv(taps_ref, first):
+            taps = taps_ref[:, at_lane]
+            lanes = slice(first, first + lane)
+            return (
+                taps[0:1, :] * up_tile[pad - 2 : pad - 2 + tokens, lanes]
+                + taps[1:2, :] * up_tile[pad - 1 : pad - 1 + tokens, lanes]
+                + taps[2:3, :] * up_tile[pad : pad + tokens, lanes]
+            )
+
+        act = jax.nn.silu(conv(gate_taps_ref, 0)) * conv(value_taps_ref, lane)
+        hidden[:, at_lane] = act.astype(jnp.bfloat16)
+
+    @pl.loop(jnp.minimum(reached + tiles, early), early)
+    def _(n):
+        tick(n)
+
+    def owner_of(i):
+        k = i // 2
+        j = lax.rem(i, 2)
+        away = j * (half + k) + (1 - j) * lax.rem(half - k, half)
+        return index(place - away)
+
+    @pl.loop(0, half)
+    def _(k):
+        for m in range(down_pieces):
+            tick(early + k * down_pieces + m)
+
+        @pl.when(k == half - 1)
+        def _():
+            for m in range(down_pieces):
+                for w in range(2):
+                    down_hop(w, count - 2, m).wait_recv()
+
+        for j in range(2):
+            i = 2 * k + j
+            owner = owner_of(i)
+            total_rows[:, columns(owner)] = product_slice(
+                hidden, lambda: full_down[owner], second_sem, i
+            )
+
+    @pl.loop(0, slices)
+    def _(i):
+        across(second_sem, i).wait_recv()
+        cols = columns(owner_of(i))
+        out_ref[:, cols] = (
+            stream[:, cols].astype(jnp.float32)
+            + (total_rows[:, cols] + far_in[i].astype(jnp.float32))
+        ).astype(out_ref.dtype)
+
+    swap.wait_send()
+
+    @pl.when(step_at + 1 < half)
+    def _():
+        hand.wait_send()
+
+    @pl.when(me + 1 < count)
+    def _():
+        edge.wait_send()
+
+    @pl.loop(0, slices)
+    def _(i):
+        pair(second_sem, i).wait_send()
+        across(second_sem, i).wait_send()
+        beside(second_sem, i).wait_send()
+
+    @pl.loop(0, row_pieces)
+    def _(p):
+        send_rows(tp, 0, p, far).wait_send()
+        send_rows(tp, 1, p, near).wait_send()
+        send_rows(far, 2, p, near).wait_send()
+
+    @pl.loop(started - 2, up_ticks)
+    def _(n):
+        up_sent(n)
+
+    @pl.loop(0, count - 1)
+    def _(t):
+        for w in range(2):
+            for m in range(down_pieces):
+                down_hop(w, t, m).wait_send()
+
+
+FIRST_TICKS = 4
+NEXT_TICKS = 2
+UP_PIECES = 4
+DOWN_PIECES = 2
+PAD_ROWS = 16
+
+
+def one_kernel_fits(rows, gate_w, down_w):
+    count = lax.axis_size("sp")
+    return (
+        lax.axis_size("tp") == 4
+        and count >= 4
+        and count % 2 == 0
+        and gate_w.shape[0] % (16 * 2 * UP_PIECES) == 0
+        and gate_w.shape[1] % 128 == 0
+        and down_w.shape[0] % (16 * 2 * DOWN_PIECES) == 0
+        and down_w.shape[1] % 128 == 0
+        and rows % 64 == 0
+    )
+
+
+def layer(q, k, v, gates, input_log, forget_log, gain, wo, residual, norm_gain, gate_w, value_w, down_w, gate_taps, value_taps):
+    count = lax.axis_size("sp")
+    heads = input_log.shape[1]
+    tokens = q.shape[0]
+    key_width = q.shape[1] // heads
+    value_width = v.shape[1] // heads
+    span = key_width + STATE_PAD
+    model = wo.shape[1]
+    rows = residual.shape[0]
+    lane = 128
+    tiles = gate_w.shape[1] // lane
+    logs = jnp.concatenate([input_log.T, forget_log.T], axis=0)
+    slices, wide = count, down_w.shape[1]
+    row_pieces = 4
+    vmem = pl.BlockSpec(memory_space=pltpu.VMEM)
+    hbm = pl.BlockSpec(memory_space=pl.ANY)
+    slots = pltpu.VMEM((slices, rows, wide), jnp.bfloat16)
+    dma = pltpu.SemaphoreType.DMA
+    return pl.pallas_call(
+        functools.partial(layer_kernel, count, heads, UP_PIECES, DOWN_PIECES),
+        out_shape=jax.ShapeDtypeStruct(residual.shape, jnp.bfloat16),
+        in_specs=[vmem] * 11 + [hbm] * 3,
+        out_specs=vmem,
+        scratch_shapes=[
+            pltpu.VMEM((tokens // BLOCK, 8, BLOCK), jnp.float32),
+            pltpu.VMEM((tokens, BLOCK), jnp.float32),
+            pltpu.VMEM((heads * span, value_width), jnp.bfloat16),
+            pltpu.VMEM((2, heads * span, value_width), jnp.bfloat16),
+            pltpu.VMEM((heads, key_width, value_width), jnp.float32),
+            pltpu.VMEM((heads, 8, key_width), jnp.float32),
+            pltpu.VMEM((heads, 8, 128), jnp.float32),
+            pltpu.VMEM((heads, key_width, value_width), jnp.float32),
+            pltpu.VMEM((heads, 8, key_width), jnp.float32),
+            pltpu.VMEM((2, heads, 8, 128), jnp.float32),
+            pltpu.VMEM((heads * span, value_width), jnp.bfloat16),
+            pltpu.VMEM((tokens, v.shape[1]), jnp.bfloat16),
+        ]
+        + [slots] * 6
+        + [
+            pltpu.VMEM((rows, model), jnp.float32),
+            pltpu.VMEM((rows, model), jnp.bfloat16),
+            pltpu.VMEM((PAD_ROWS + tokens, model), jnp.bfloat16),
+            pltpu.VMEM((tiles, model, 2 * lane), jnp.bfloat16),
+            pltpu.VMEM((count,) + down_w.shape, jnp.bfloat16),
+            pltpu.VMEM((PAD_ROWS + tokens, 2 * lane), jnp.float32),
+            pltpu.VMEM((tokens, down_w.shape[0]), jnp.bfloat16),
+            dma((2 * tiles + 1,)),
+            dma((2,)),
+            dma((2,)),
+            dma((2, UP_PIECES, count - 1)),
+            dma((2, UP_PIECES, count - 1)),
+            dma((2, DOWN_PIECES, count - 1)),
+            dma((2, DOWN_PIECES, count - 1)),
+            dma((6, slices)),
+            dma((6, slices)),
+            dma((6, row_pieces)),
+            dma((2,)),
+        ],
+        compiler_params=pltpu.CompilerParams(
+            collective_id=0, has_side_effects=True, vmem_limit_bytes=60 * 1024 * 1024
+        ),
+        cost_estimate=pl.CostEstimate(
+            flops=30_000_000_000, bytes_accessed=8 * v.size, transcendentals=0
+        ),
+    )(
+        logs,
+        q,
+        k,
+        v,
+        gates,
+        gain,
+        wo,
+        residual,
+        norm_gain[None, :],
+        gate_taps,
+        value_taps,
+        gate_w,
+        value_w,
+        down_w,
+    )
+
+
 def local(
     residual_entry_input,
     query_matrix_rows,
@@ -536,6 +1289,24 @@
     input_log, forget_log = gate_log_values(
         input_gate_logits, forget_gate_logits, forget_decay_offset
     )
+    if one_kernel_fits(residual_entry_input.shape[0], gate_up_weight, down_projection_weight):
+        return layer(
+            query_matrix_rows,
+            key_matrix_rows,
+            value_matrix_rows,
+            output_gate_logits,
+            input_log,
+            forget_log,
+            head_norm_gain,
+            cell_output_weight,
+            residual_entry_input,
+            feedforward_norm_gain,
+            gate_up_weight,
+            value_up_weight,
+            down_projection_weight,
+            gate_filter_taps,
+            value_filter_taps,
+        )
     whole_gate = lax.all_gather(gate_up_weight, "sp", axis=0, tiled=True)
     whole_down = lax.all_gather(down_projection_weight, "sp", axis=1, tiled=True)
     gated_rows = cell(

time: 324 us -> 208 us (0.64)
  Pallas kernels: 264 us -> 203 us
  matrix products: 21.4 us -> 0 us
  between operations: 13.8 us -> 0.01 us
  other arithmetic: 10.2 us -> 1.39 us
  local copies, waits for them, and re-layouts: 10.8 us -> 2.3 us
    pallas_call x5 -> x1, Pallas kernels: 264 us -> 203 us  [layer(): pl.pallas_call(functools.partial(layer_kernel, count, heads, UP_PIECES, D...]
    dot_general x5 -> x0, matrix products: 21.4 us -> none  [the longest x1 10.7 us: local(): up_gate = jnp.dot(window, whole_gate, preferred_element_type=jnp.float32)]
    convert_element_type x7 -> x0, other arithmetic: 6.56 us -> none  [the longest x1 4.69 us: local(): hidden = (jax.nn.silu(conv_g) * conv_v).astype(jnp.bfloat16)]
    mul x2 -> x0, local copies, waits for them, and re-layouts: 3.64 us -> none  [cell(): k.reshape(tokens, heads, key_width).astype(jnp.float32)]
  transfers between devices with their start and end apart: 3 -> 0, of which waited for: 0 -> 0; matrix products, arithmetic and copies ran while one was open for 12% -> 0% of each run, Pallas kernels for 71% -> 0%
where the time goes in v1:
time: 208 us; the launch traced here: 207 us
  Pallas kernels  203 us (98%)
  local copies, waits for them, and re-layouts  2.3 us (1%)
    pallas_call x1, Pallas kernels, layer(): pl.pallas_call(functools.partial(layer_kernel, count, heads, UP_PIECES, D...  203 us

profile of v1, /device:TPU:29, one launch (start us, length us, event | category | flops | bytes accessed | tf_op | source)
XLA Modules:
  0.0 206.8 jit_solution(17604682573409376391)
XLA Ops:
  0.0 0.8 fusion.2
  0.8 0.6 pad_maximum_fusion.logs_ref
  1.4 203.1 %shard_map.154 = bf16[256,2048]{1,0:T(8,128)(2,1)} custom-call(f32[4,1024]{1,0:T(4,128)} %pad_maximum_fusion.logs_ref, bf16[1024,256]{1,0:T(8,128)(2,1)} %q_ref.1, bf16[1024,256]{1,0:T(8,128)(2,1)} %k_ref.1, bf16[1024,512]{1,0:T(8,128)(2,1)} %v_ref.1, bf16[1024,512]{1,0:T(8,128)(2,1)} %gate_ref.1, f32[2,256]{1,0:T(2,128)} %gain_ref.1, ...), custom_call_target="tpu_custom_call" | custom-call | flops 30000001024 | bytes 4194304 | tf_op jit(solution)/shard_map/pallas_call | solution.py:1207
  204.4 2.3 %copy.18 = bf16[256,2048]{1,0:T(8,128)(2,1)} copy(bf16[256,2048]{1,0:T(8,128)(2,1)} %shard_map.154) | data formatting | bytes 2097152

commit v2 on v1

--- a/solution.py
+++ b/solution.py
@@ -536,11 +536,11 @@
     v_ref,
     gate_ref,
     gain_ref,
-    wo_ref,
     residual_ref,
     norm_gain_ref,
     gate_taps_ref,
     value_taps_ref,
+    wo_ref,
     gate_w_ref,
     value_w_ref,
     down_w_ref,
@@ -557,137 +557,199 @@
     pair_level,
     handed,
     gated,
-    pair_out,
-    pair_in,
-    far_out,
-    far_in,
-    near_out,
-    near_in,
+    mine,
+    wo_full,
+    middle,
+    give_up,
+    give_down,
+    full_up,
+    full_down,
     total_rows,
     stream,
     group,
-    full_up,
-    full_down,
     up_tile,
     hidden,
+    pair_out,
+    pair_in,
+    second_out,
+    second_in,
+    third_out,
+    third_in,
+    kept,
     load_sem,
+    wo_sem,
+    give_sem,
     state_send,
     state_recv,
     up_send,
     up_recv,
     down_send,
     down_recv,
-    first_sem,
-    second_sem,
-    rows_sem,
+    block_send,
+    block_recv,
+    rows_send,
+    rows_recv,
+    sum_send,
+    sum_recv,
     edge_sem,
 ):
     me = lax.axis_index("sp")
     tp = lax.axis_index("tp")
-    near = tp + 1 - 2 * lax.rem(tp, 2)
+    core = lax.rem(tp, 2)
+    chip = tp // 2
+    near = tp + 1 - 2 * core
     far = lax.rem(tp + 2, 4)
     opposite = lax.rem(near + 2, 4)
     odd = lax.rem(me, 2)
-    half = count // 2
-    place = me // 2 + odd * (count - 1 - 2 * (me // 2))
-    tiles = full_up.shape[0]
-    up_rows = full_up.shape[1] // count
-    up_step = up_rows // (2 * up_pieces)
-    down_step = full_down.shape[1] // (2 * down_pieces)
-    lane = full_up.shape[2] // 2
+    partner = me + 1 - 2 * odd
+    line = count // 2
+    place = me // 2
+    model = full_up.shape[0]
+    lane = 128
+    up_rows = model // count
+    up_step = 2 * up_rows // up_pieces
+    half_width = full_down.shape[1]
+    tiles = half_width // lane
+    rest = half_width - tiles * lane
+    wide = full_down.shape[2]
+    down_step = 2 * half_width // down_pieces
 
     barrier = pltpu.get_barrier_semaphore()
-    for d in range(1, count):
-        pl.semaphore_signal(
-            barrier, inc=1, device_id={"sp": lax.rem(me + d, count)}, device_id_type=MESH
-        )
-    for other in (near, far):
+    for other in (near, far, opposite):
         pl.semaphore_signal(barrier, inc=1, device_id={"tp": other}, device_id_type=MESH)
+    for other in (partner, lax.rem(me + 2, count), lax.rem(me + count - 2, count)):
+        pl.semaphore_signal(barrier, inc=1, device_id={"sp": other}, device_id_type=MESH)
 
     own_up = pl.ds(pl.multiple_of(me * up_rows, up_rows), up_rows)
+    wo_rows = wo_ref.shape[0]
+    wo_own = pl.ds(pl.multiple_of(tp * wo_rows, wo_rows), wo_rows)
     loads = []
+
+    def load(src, dst):
+        loads.append(pltpu.make_async_copy(src, dst, load_sem.at[len(loads)]))
+
+    shift = tiles * lane + 2 * rest
     for i in range(tiles):
         for a, w_ref in enumerate((gate_w_ref, value_w_ref)):
-            loads.append(
-                pltpu.make_async_copy(
-                    w_ref.at[:, pl.ds(i * lane, lane)],
-                    full_up.at[i, own_up, pl.ds(a * lane, lane)],
-                    load_sem.at[2 * i + a],
-                )
-            )
-    down_load = pltpu.make_async_copy(down_w_ref, full_down.at[me], load_sem.at[2 * tiles])
-    for load in loads:
-        load.start()
-    down_load.start()
-
-    pl.semaphore_wait(barrier, count + 1)
-
-    step_at = me // 2
-    swap = pltpu.make_async_remote_copy(
-        src_ref=state_ref,
-        dst_ref=held.at[0],
-        send_sem=state_send.at[0],
-        recv_sem=state_recv.at[0],
-        device_id={"sp": me + 1 - 2 * odd},
-        device_id_type=MESH,
+            lanes = pl.ds((2 * i + a) * lane, lane)
+            for to, y in ((full_up.at[own_up, lanes], odd), (give_up.at[:, lanes], 1 - odd)):
+                at = pl.multiple_of(y * shift + i * lane, lane)
+                load(w_ref.at[:, pl.ds(at, lane)], to)
+    for a, w_ref in enumerate((gate_w_ref, value_w_ref)):
+        load(w_ref.at[:, pl.ds(tiles * lane, lane)], middle.at[a])
+    for to, y in ((full_down.at[me], odd), (give_down, 1 - odd)):
+        at = pl.multiple_of(y * shift, rest)
+        load(down_w_ref.at[pl.ds(at, tiles * lane)], to.at[pl.ds(0, tiles * lane)])
+        at = pl.multiple_of(tiles * lane + y * rest, rest)
+        load(down_w_ref.at[pl.ds(at, rest)], to.at[pl.ds(tiles * lane, rest)])
+    load(wo_ref, wo_full.at[wo_own])
+    for one in loads:
+        one.start()
+    pl.semaphore_wait(barrier, 6)
+    for one in loads:
+        one.wait()
+
+    def remote(src, dst, send_sem, recv_sem, **to):
+        return pltpu.make_async_remote_copy(
+            src_ref=src,
+            dst_ref=dst,
+            send_sem=send_sem,
+            recv_sem=recv_sem,
+            device_id=to,
+            device_id_type=MESH,
+        )
+
+    at_lane = lax.broadcasted_iota(jnp.int32, (up_rows, lane), 1)
+    first_half = at_lane < rest
+
+    def halves_of(g, v, low):
+        a = jnp.where(low, g, pltpu.roll(v, rest, 1))
+        b = jnp.where(low, pltpu.roll(g, rest, 1), v)
+        return a, b
+
+    mid_a, mid_b = halves_of(
+        middle[0].astype(jnp.float32), middle[1].astype(jnp.float32), first_half
     )
-    hand = pltpu.make_async_remote_copy(
-        src_ref=handed,
-        dst_ref=held.at[1],
-        send_sem=state_send.at[1],
-        recv_sem=state_recv.at[1],
-        device_id={"sp": lax.rem(me + 2, count)},
-        device_id_type=MESH,
-    )
-    def index(position):
-        position = lax.rem(position + 2 * count, count)
-        back = position // half
-        return (1 - back) * 2 * position + back * (2 * (count - 1 - position) + 1)
-
-    ways = (1, -1)
+    tail = slice(2 * tiles * lane, 2 * tiles * lane + lane)
+    full_up[own_up, tail] = jnp.where(odd == 0, mid_a, mid_b).astype(jnp.bfloat16)
+    give_up[:, tail] = jnp.where(odd == 0, mid_b, mid_a).astype(jnp.bfloat16)
+
+    give_step = up_rows // 2
+
+    def give_rows(p):
+        at = pl.multiple_of(me * up_rows + p * give_step, give_step)
+        return remote(
+            give_up.at[pl.ds(p * give_step, give_step)],
+            full_up.at[pl.ds(at, give_step)],
+            give_sem.at[0, p],
+            give_sem.at[1, p],
+            sp=partner,
+        )
+
+    give_cols = remote(give_down, full_down.at[me], give_sem.at[0, 2], give_sem.at[1, 2], sp=partner)
+    wo_step = wo_rows // 2
+
+    def wo_copy(kind, owner, p, target):
+        at = pl.multiple_of(owner * wo_rows + p * wo_step, wo_step)
+        part = wo_full.at[pl.ds(at, wo_step)]
+        return remote(part, part, wo_sem.at[0, kind, p], wo_sem.at[1, kind, p], tp=target)
+
+    def source(w, t):
+        return place - t if w == 0 else place + t
+
+    def has(w, t):
+        return place >= t if w == 0 else place + t < line
+
+    def sends(w, t):
+        onward = place + 1 < line if w == 0 else place > 0
+        return has(w, t) & onward & (t < line - 1)
+
+    def beyond(w):
+        return lax.rem(me + 2, count) if w == 0 else lax.rem(me + count - 2, count)
 
     def up_hop(w, t, m):
-        owner = index(place - ways[w] * t)
-        row = owner * up_rows + (w * up_pieces + m) * up_step
-        part = full_up.at[:, pl.ds(pl.multiple_of(row, up_step), up_step), :]
-        return pltpu.make_async_remote_copy(
-            src_ref=part,
-            dst_ref=part,
-            send_sem=up_send.at[w, m, t],
-            recv_sem=up_recv.at[w, m, t],
-            device_id={"sp": index(place + ways[w])},
-            device_id_type=MESH,
-        )
+        at = source(w, t) * 2 * up_rows + lax.rem(m + odd * (up_pieces // 2), up_pieces) * up_step
+        part = full_up.at[pl.ds(pl.multiple_of(at, up_step), up_step)]
+        return remote(part, part, up_send.at[w, t, m], up_recv.at[w, t, m], sp=beyond(w))
 
     def down_hop(w, t, m):
-        owner = index(place - ways[w] * t)
-        row = (w * down_pieces + m) * down_step
-        part = full_down.at[owner, pl.ds(pl.multiple_of(row, down_step), down_step), :]
-        return pltpu.make_async_remote_copy(
-            src_ref=part,
-            dst_ref=part,
-            send_sem=down_send.at[w, m, t],
-            recv_sem=down_recv.at[w, m, t],
-            device_id={"sp": index(place + ways[w])},
-            device_id_type=MESH,
-        )
-
-    up_ticks = (count - 1) * up_pieces
-    all_ticks = up_ticks + (count - 1) * down_pieces
+        each = down_pieces // 2
+        owner = source(w, t) * 2 + lax.rem(m // each + odd, 2)
+        at = lax.rem(m, each) * down_step
+        part = full_down.at[owner, pl.ds(pl.multiple_of(at, down_step), down_step)]
+        return remote(part, part, down_send.at[w, t, m], down_recv.at[w, t, m], sp=beyond(w))
+
+    up_ticks = line * up_pieces
+    all_ticks = up_ticks + line * down_pieces
 
     def move(hop, pieces, n):
         t = n // pieces
         m = lax.rem(n, pieces)
         for w in range(2):
 
-            @pl.when(t > 0)
+            @pl.when(has(w, t) & (t > 0))
             def _():
                 hop(w, t - 1, m).wait_recv()
 
-            hop(w, t, m).start()
+            @pl.when(sends(w, t))
+            def _():
+                hop(w, t, m).start()
 
     def up_tick(n):
+        for p in range(2):
+
+            @pl.when(n == up_pieces // 2 + p * (up_pieces // 4))
+            def _():
+                give_rows(p).wait_recv()
+
         move(up_hop, up_pieces, n)
+
+    def down_tick(n):
+        @pl.when(n == down_pieces // 2)
+        def _():
+            give_cols.wait_recv()
+
+        move(down_hop, down_pieces, n)
 
     def tick(n):
         @pl.when(n < up_ticks)
@@ -696,21 +758,28 @@
 
         @pl.when((n >= up_ticks) & (n < all_ticks))
         def _():
-            move(down_hop, down_pieces, n - up_ticks)
+            down_tick(n - up_ticks)
 
     def up_sent(n):
+        t = n // up_pieces
         for w in range(2):
-            up_hop(w, n // up_pieces, lax.rem(n, up_pieces)).wait_send()
-
-    for load in loads:
-        load.wait()
-    down_load.wait()
+
+            @pl.when(sends(w, t))
+            def _():
+                up_hop(w, t, lax.rem(n, up_pieces)).wait_send()
+
+    give_rows(0).start()
+    for p in range(2):
+        wo_copy(0, tp, p, far).start()
+        wo_copy(1, tp, p, near).start()
     for n in range(2):
         up_tick(n)
 
     key_width = memory.shape[1]
     value_width = memory.shape[2]
     span = key_width + STATE_PAD
+    swap = remote(state_ref, held.at[0], state_send.at[0], state_recv.at[0], sp=partner)
+    hand = remote(handed, held.at[1], state_send.at[1], state_recv.at[1], sp=beyond(0))
 
     def read_state(ref, h):
         low = h * span
@@ -819,6 +888,8 @@
             own_total[h : h + 1, :],
         )
     swap.start()
+    give_rows(1).start()
+    give_cols.start()
     swap.wait_recv()
 
     @pl.when(odd == 0)
@@ -839,7 +910,7 @@
             keep((pair_memory, pair_normer, pair_level.at[0]), h, out)
             pair_level[1, h] = jnp.broadcast_to(total_a + total_b, pair_level.shape[2:])
 
-    started = jnp.minimum(FIRST_TICKS + NEXT_TICKS * step_at, up_ticks)
+    started = jnp.minimum(FIRST_TICKS + NEXT_TICKS * place, up_ticks)
 
     @pl.loop(2, started)
     def _(n):
@@ -850,14 +921,14 @@
     normer[...] = jnp.zeros_like(normer)
     running[...] = jnp.full(running.shape, neg_large, jnp.float32)
 
-    @pl.when(step_at > 0)
+    @pl.when(place > 0)
     def _():
         hand.wait_recv()
         for h in range(heads):
             mem, parts, level, total = read_state(held.at[1], h)
             keep(carried_refs, h, (mem, parts, level))
 
-    @pl.when(step_at + 1 < half)
+    @pl.when(place + 1 < line)
     def _():
         for h in range(heads):
             mem, norm, level = join(
@@ -879,10 +950,30 @@
 
     scale = key_width ** (-0.5)
     causal = at_col <= at_row
+    size = residual_ref.shape[0]
+    per = size // length
+
+    def block_copy(j, sender):
+        at = pl.multiple_of(lax.rem(j, per) * length, length)
+        width = gated.shape[1]
+        return remote(
+            gated.at[pl.ds(pl.multiple_of(j * length, length), length)],
+            mine.at[sender, pl.ds(at, length)],
+            block_send.at[j],
+            block_recv.at[sender, lax.rem(j, per)],
+            tp=j // per,
+        )
 
     @pl.loop(0, blocks)
     def _(j):
         tick(started + j)
+
+        @pl.when(j == blocks - 2)
+        def _():
+            for p in range(2):
+                wo_copy(0, far, p, far).wait_recv()
+                wo_copy(2, far, p, near).start()
+
         rows = pl.ds(pl.multiple_of(j * length, length), length)
         lanes = rows_ref[j]
         cols = cols_ref[rows, :]
@@ -936,82 +1027,58 @@
             )
             running[h] = jnp.broadcast_to(last + total, running.shape[1:])
 
-    size = residual_ref.shape[0]
-    slices = pair_out.shape[0]
-    wide = pair_out.shape[2]
+        @pl.when(j // per == tp)
+        def _():
+            at = pl.multiple_of(lax.rem(j, per) * length, length)
+            mine[tp, pl.ds(at, length), :] = gated[rows, :]
+
+        @pl.when(j // per != tp)
+        def _():
+            block_copy(j, tp).start()
+
+    reached = started + blocks
+    for p in range(2):
+        wo_copy(1, near, p, near).wait_recv()
+        wo_copy(2, opposite, p, near).wait_recv()
+
+    @pl.loop(0, 4)
+    def _(s):
+        tick(reached + s)
+
+        @pl.when(s != tp)
+        def _():
+            for p in range(per):
+                block_copy(tp * per + p, s).wait_recv()
+
+    reached = reached + 4
 
     def columns(i):
         return pl.ds(pl.multiple_of(i * wide, wide), wide)
 
-    def exchange(src, dst, sems, kind, i, target):
-        return pltpu.make_async_remote_copy(
-            src_ref=src.at[i],
-            dst_ref=dst.at[i],
-            send_sem=sems.at[2 * kind, i],
-            recv_sem=sems.at[2 * kind + 1, i],
-            device_id={"tp": target},
-            device_id_type=MESH,
-        )
-
-    def pair(sems, i):
-        return exchange(pair_out, pair_in, sems, 0, i, near)
-
-    def across(sems, i):
-        return exchange(far_out, far_in, sems, 1, i, far)
-
-    def beside(sems, i):
-        return exchange(near_out, near_in, sems, 2, i, near)
-
-    def product_slice(x_ref, weight, sems, i):
-        def term(owner):
-            rows = pl.ds(pl.multiple_of(owner * size, size), size)
-            return jnp.dot(x_ref[rows, :], weight(), preferred_element_type=jnp.float32)
-
-        pair_out[i] = term(opposite).astype(jnp.bfloat16)
-        pair(sems, i).start()
-        onward = term(far)
-        near_out[i] = term(near).astype(jnp.bfloat16)
-        beside(sems, i).start()
-        pair(sems, i).wait_recv()
-        far_out[i] = (onward + pair_in[i].astype(jnp.float32)).astype(jnp.bfloat16)
-        across(sems, i).start()
-        own = term(tp)
-        beside(sems, i).wait_recv()
-        return own + near_in[i].astype(jnp.float32)
-
-    @pl.loop(0, slices)
+    @pl.loop(0, model // wide)
     def _(i):
-        tick(started + blocks + i)
-        total_rows[:, columns(i)] = product_slice(
-            gated, lambda: wo_ref[:, columns(i)], first_sem, i
-        )
-
-    @pl.loop(0, slices)
-    def _(i):
-        across(first_sem, i).wait_recv()
-        total_rows[:, columns(i)] += far_in[i].astype(jnp.float32)
-
-    pad = group.shape[0] - 4 * size
-    row_pieces = rows_sem.shape[1]
+        total = jnp.zeros((size, wide), jnp.float32)
+        for s in range(4):
+            total += jnp.dot(
+                mine[s],
+                wo_full[s * wo_rows : (s + 1) * wo_rows, columns(i)],
+                preferred_element_type=jnp.float32,
+            )
+        total_rows[:, columns(i)] = total
+
+    pad = PAD_ROWS
+    tokens = 8 * size
+    row_pieces = rows_send.shape[1]
     row_step = size // row_pieces
 
-    def at(owner, p):
-        row = pad + owner * size + p * row_step
-        return group.at[pl.ds(pl.multiple_of(row, pad), row_step)]
-
-    def send_rows(owner, kind, p, target):
-        return pltpu.make_async_remote_copy(
-            src_ref=at(owner, p),
-            dst_ref=at(owner, p),
-            send_sem=rows_sem.at[2 * kind, p],
-            recv_sem=rows_sem.at[2 * kind + 1, p],
-            device_id={"tp": target},
-            device_id_type=MESH,
-        )
-
-    @pl.when(me == 0)
+    def row_copy(kind, y, owner, p, **to):
+        at = pad + (y * 4 + owner) * size + p * row_step
+        part = group.at[pl.ds(pl.multiple_of(at, pad), row_step)]
+        return remote(part, part, rows_send.at[kind, p], rows_recv.at[kind, p], **to)
+
+    @pl.when(place == 0)
     def _():
-        group[0:pad, :] = jnp.zeros((pad, group.shape[1]), group.dtype)
+        group[0:pad, :] = jnp.zeros((pad, model), group.dtype)
 
     @pl.loop(0, row_pieces)
     def _(p):
@@ -1022,153 +1089,269 @@
         stream[rows, :] = rounded
         x = rounded.astype(jnp.float32)
         normed = x * lax.rsqrt(jnp.mean(x * x, axis=-1, keepdims=True) + eps) * norm_gain_ref[...]
-        row = pad + tp * size + p * row_step
-        group[pl.ds(pl.multiple_of(row, pad), row_step), :] = normed.astype(jnp.bfloat16)
-        send_rows(tp, 0, p, far).start()
-        send_rows(tp, 1, p, near).start()
+        at = pl.multiple_of(pad + (odd * 4 + tp) * size + p * row_step, pad)
+        group[pl.ds(at, row_step), :] = normed.astype(jnp.bfloat16)
+        row_copy(0, odd, tp, p, tp=far).start()
+        row_copy(2, odd, tp, p, sp=partner).start()
+        row_copy(1, odd, tp, p, tp=near).start()
 
     @pl.loop(0, row_pieces)
     def _(p):
-        tick(started + blocks + slices + p)
-        send_rows(far, 0, p, far).wait_recv()
-        send_rows(far, 2, p, near).start()
+        tick(reached + 2 * p)
+        row_copy(0, odd, far, p, tp=far).wait_recv()
+        row_copy(3, odd, far, p, tp=near).start()
+
+        @pl.when(lax.rem(p, 2) == 0)
+        def _():
+            row_copy(6, odd, far, p, sp=partner).start()
+
+        tick(reached + 2 * p + 1)
+        row_copy(2, 1 - odd, tp, p, sp=partner).wait_recv()
+        row_copy(4, 1 - odd, tp, p, tp=near).start()
+
+        @pl.when(lax.rem(p, 2) == 1)
+        def _():
+            row_copy(6, 1 - odd, tp, p, tp=far).start()
+
+    reached = reached + 2 * row_pieces
 
     @pl.loop(0, row_pieces)
     def _(p):
-        send_rows(near, 1, p, near).wait_recv()
-        send_rows(opposite, 2, p, near).wait_recv()
-
-    edge = pltpu.make_async_remote_copy(
-        src_ref=group.at[pl.ds(4 * size, pad)],
-        dst_ref=group.at[pl.ds(0, pad)],
-        send_sem=edge_sem.at[0],
-        recv_sem=edge_sem.at[1],
-        device_id={"sp": lax.rem(me + 1, count)},
-        device_id_type=MESH,
+        tick(reached + p)
+        row_copy(6, 1 - odd, far, p, sp=partner).wait_recv()
+        row_copy(5, 1 - odd, far, p, tp=near).start()
+        row_copy(1, odd, near, p, tp=near).wait_recv()
+        row_copy(3, odd, opposite, p, tp=near).wait_recv()
+        row_copy(4, 1 - odd, near, p, tp=near).wait_recv()
+
+    reached = reached + row_pieces
+
+    @pl.loop(0, row_pieces)
+    def _(p):
+        row_copy(5, 1 - odd, opposite, p, tp=near).wait_recv()
+
+    edge = remote(
+        group.at[pl.ds(tokens, pad)],
+        group.at[pl.ds(0, pad)],
+        edge_sem.at[0],
+        edge_sem.at[1],
+        sp=beyond(0),
     )
 
-    @pl.when(me + 1 < count)
+    @pl.when(place + 1 < line)
     def _():
         edge.start()
 
-    reached = jnp.maximum(started + blocks + slices + row_pieces, up_ticks)
-
-    @pl.loop(jnp.minimum(started + blocks + slices + row_pieces, up_ticks), up_ticks)
+    @pl.loop(jnp.minimum(reached, up_ticks), up_ticks)
     def _(n):
         up_tick(n)
 
-    for m in range(up_pieces):
-        for w in range(2):
-            up_hop(w, count - 2, m).wait_recv()
-
-    @pl.when(me > 0)
-    def _():
-        edge.wait_recv()
-
-    @pl.loop(0, slices)
-    def _(i):
-        pair(first_sem, i).wait_send()
-        across(first_sem, i).wait_send()
-        beside(first_sem, i).wait_send()
-
-    early = up_ticks + half * down_pieces
-
-    @pl.loop(0, tiles)
-    def _(i):
-        @pl.when(reached + i < early)
-        def _():
-            tick(reached + i)
-
-        up_tile[...] = jnp.dot(group[...], full_up[i], preferred_element_type=jnp.float32)
-        tokens = 4 * size
-        at_lane = pl.ds(pl.multiple_of(i * lane, lane), lane)
-
-        def conv(taps_ref, first):
-            taps = taps_ref[:, at_lane]
-            lanes = slice(first, first + lane)
+    reached = jnp.maximum(reached, up_ticks)
+    early = up_ticks + 2 * down_pieces
+    parts = 4
+    part_rows = tokens // parts
+
+    def silu(a):
+        return a * jax.nn.sigmoid(a)
+
+    @pl.loop(0, parts)
+    def _(b):
+        part = lax.rem(b + 1, parts)
+        at = pl.multiple_of(part * part_rows, part_rows)
+        window = pl.ds(at, part_rows + pad)
+        outs = pl.ds(at, part_rows)
+
+        @pl.when((b == parts - 1) & (place > 0))
+        def _():
+            edge.wait_recv()
+
+        def conv(taps, width):
             return (
-                taps[0:1, :] * up_tile[pad - 2 : pad - 2 + tokens, lanes]
-                + taps[1:2, :] * up_tile[pad - 1 : pad - 1 + tokens, lanes]
-                + taps[2:3, :] * up_tile[pad : pad + tokens, lanes]
-            )
-
-        act = jax.nn.silu(conv(gate_taps_ref, 0)) * conv(value_taps_ref, lane)
-        hidden[:, at_lane] = act.astype(jnp.bfloat16)
-
-    @pl.loop(jnp.minimum(reached + tiles, early), early)
+                taps[0:1, :] * up_tile[pad - 2 : pad - 2 + part_rows, width]
+                + taps[1:2, :] * up_tile[pad - 1 : pad - 1 + part_rows, width]
+                + taps[2:3, :] * up_tile[pad : pad + part_rows, width]
+            )
+
+        @pl.loop(0, tiles)
+        def _(i):
+            n = reached + b * (tiles + 1) + i
+
+            @pl.when(n < early)
+            def _():
+                tick(n)
+
+            lanes = pl.ds(pl.multiple_of(i * 2 * lane, 2 * lane), 2 * lane)
+            up_tile[...] = jnp.dot(
+                group[window, :], full_up[:, lanes], preferred_element_type=jnp.float32
+            )
+            taps_at = pl.ds(pl.multiple_of(odd * shift + i * lane, lane), lane)
+            act = silu(conv(gate_taps_ref[:, taps_at], slice(0, lane))) * conv(
+                value_taps_ref[:, taps_at], slice(lane, 2 * lane)
+            )
+            hidden[outs, pl.ds(pl.multiple_of(i * lane, lane), lane)] = act.astype(jnp.bfloat16)
+
+        n = reached + b * (tiles + 1) + tiles
+
+        @pl.when(n < early)
+        def _():
+            tick(n)
+
+        up_tile[:, 0:lane] = jnp.dot(
+            group[window, :], full_up[:, tail], preferred_element_type=jnp.float32
+        )
+        mid = slice(tiles * lane, (tiles + 1) * lane)
+        low = lax.broadcasted_iota(jnp.int32, (3, lane), 1) < rest
+        taps_a, taps_b = halves_of(gate_taps_ref[:, mid], value_taps_ref[:, mid], low)
+        both = conv(jnp.where(odd == 0, taps_a, taps_b), slice(0, lane))
+        act = silu(both) * pltpu.roll(both, rest, 1)
+        hidden[outs, tiles * lane : tiles * lane + rest] = act[:, :rest].astype(jnp.bfloat16)
+
+    @pl.loop(jnp.minimum(reached + parts * (tiles + 1), early), early)
     def _(n):
         tick(n)
 
-    def owner_of(i):
-        k = i // 2
-        j = lax.rem(i, 2)
-        away = j * (half + k) + (1 - j) * lax.rem(half - k, half)
-        return index(place - away)
-
-    @pl.loop(0, half)
-    def _(k):
-        for m in range(down_pieces):
-            tick(early + k * down_pieces + m)
-
-        @pl.when(k == half - 1)
-        def _():
-            for m in range(down_pieces):
-                for w in range(2):
-                    down_hop(w, count - 2, m).wait_recv()
-
-        for j in range(2):
-            i = 2 * k + j
-            owner = owner_of(i)
-            total_rows[:, columns(owner)] = product_slice(
-                hidden, lambda: full_down[owner], second_sem, i
-            )
-
-    @pl.loop(0, slices)
-    def _(i):
-        across(second_sem, i).wait_recv()
-        cols = columns(owner_of(i))
+    both_sides = jnp.minimum(place, line - 1 - place)
+
+    def away(k):
+        return jnp.where(k <= 2 * both_sides, (k + 1) // 2, k - both_sides)
+
+    def unit(k):
+        rising = jnp.where(place < line - 1 - place, 1, -1)
+        way = jnp.where(k <= 2 * both_sides, 1 - 2 * lax.rem(k, 2), rising)
+        return place + way * away(k)
+
+    def sum_copy(stage, i, parity):
+        src, dst = ((pair_out, pair_in), (second_out, second_in), (third_out, third_in))[stage]
+        if stage == 0:
+            to = {"tp": near}
+        elif (stage == 1) == (parity == 0):
+            to = {"tp": far}
+        else:
+            to = {"sp": partner}
+        return remote(src.at[i], dst.at[i], sum_send.at[stage, i], sum_recv.at[stage, i], **to)
+
+    def term(i, y, owner):
+        rows = pl.ds(pl.multiple_of((y * 4 + owner) * size, size), size)
+        return jnp.dot(hidden[rows, :], full_down[i], preferred_element_type=jnp.float32)
+
+    def first_stage(i, parity):
+        for y in range(2):
+            for x in range(2):
+                pair_out[i, 2 * y + x] = term(i, y, 2 * x + 1 - core).astype(jnp.bfloat16)
+        sum_copy(0, i, parity).start()
+
+    def second_stage(i, parity):
+        for a in range(2):
+            y, x = (a, 1 - chip) if parity == 0 else (1 - odd, a)
+            pair_in_at = 2 * y + x
+            second_out[i, a] = term(i, y, 2 * x + core).astype(jnp.bfloat16)
+        for a in range(2):
+            y, x = (a, chip) if parity == 0 else (odd, a)
+            kept[i, a] = term(i, y, 2 * x + core)
+        sum_copy(0, i, parity).wait_recv()
+        for a in range(2):
+            y, x = (a, 1 - chip) if parity == 0 else (1 - odd, a)
+            second_out[i, a] = (
+                second_out[i, a].astype(jnp.float32) + pair_in[i, 2 * y + x].astype(jnp.float32)
+            ).astype(jnp.bfloat16)
+        sum_copy(1, i, parity).start()
+        for a in range(2):
+            y, x = (a, chip) if parity == 0 else (odd, a)
+            kept[i, a] += pair_in[i, 2 * y + x].astype(jnp.float32)
+
+    def third_stage(i, parity):
+        sum_copy(1, i, parity).wait_recv()
+        own = odd if parity == 0 else chip
+        third_out[i] = (kept[i, 1 - own] + second_in[i, 1 - own].astype(jnp.float32)).astype(
+            jnp.bfloat16
+        )
+        sum_copy(2, i, parity).start()
+        total_rows[:, columns(i)] = kept[i, own] + second_in[i, own].astype(jnp.float32)
+
+    def last_stage(i, parity):
+        sum_copy(2, i, parity).wait_recv()
+        cols = columns(i)
         out_ref[:, cols] = (
             stream[:, cols].astype(jnp.float32)
-            + (total_rows[:, cols] + far_in[i].astype(jnp.float32))
+            + (total_rows[:, cols] + third_in[i].astype(jnp.float32))
         ).astype(out_ref.dtype)
 
+    def until(k):
+        return up_ticks + down_pieces * (jnp.maximum(away(k), 1) + 1)
+
+    @pl.loop(0, line)
+    def _(k):
+        @pl.when(k > 0)
+        def _():
+            @pl.loop(until(k - 1), until(k))
+            def _(n):
+                tick(n)
+
+        for parity in range(2):
+            first_stage(2 * unit(k) + parity, parity)
+        for parity in range(2):
+            second_stage(2 * unit(k) + parity, parity)
+
+        @pl.when(k > 0)
+        def _():
+            for parity in range(2):
+                third_stage(2 * unit(k - 1) + parity, parity)
+
+    for parity in range(2):
+        third_stage(2 * unit(line - 1) + parity, parity)
+
+    @pl.loop(0, line)
+    def _(k):
+        for parity in range(2):
+            last_stage(2 * unit(k) + parity, parity)
+
     swap.wait_send()
 
-    @pl.when(step_at + 1 < half)
+    @pl.when(place + 1 < line)
     def _():
         hand.wait_send()
-
-    @pl.when(me + 1 < count)
-    def _():
         edge.wait_send()
 
-    @pl.loop(0, slices)
-    def _(i):
-        pair(second_sem, i).wait_send()
-        across(second_sem, i).wait_send()
-        beside(second_sem, i).wait_send()
+    for p in range(2):
+        give_rows(p).wait_send()
+        for kind in range(3):
+            wo_copy(kind, tp, p, near).wait_send()
+    give_cols.wait_send()
+
+    @pl.loop(0, blocks)
+    def _(j):
+        @pl.when(j // per != tp)
+        def _():
+            block_copy(j, tp).wait_send()
 
     @pl.loop(0, row_pieces)
     def _(p):
-        send_rows(tp, 0, p, far).wait_send()
-        send_rows(tp, 1, p, near).wait_send()
-        send_rows(far, 2, p, near).wait_send()
+        for kind in range(7):
+            row_copy(kind, odd, tp, p, tp=near).wait_send()
+
+    @pl.loop(0, count)
+    def _(i):
+        for stage in range(3):
+            sum_copy(stage, i, 0).wait_send()
 
     @pl.loop(started - 2, up_ticks)
     def _(n):
         up_sent(n)
 
-    @pl.loop(0, count - 1)
+    @pl.loop(0, line - 1)
     def _(t):
         for w in range(2):
-            for m in range(down_pieces):
-                down_hop(w, t, m).wait_send()
+
+            @pl.when(sends(w, t))
+            def _():
+                for m in range(down_pieces):
+                    down_hop(w, t, m).wait_send()
 
 
 FIRST_TICKS = 4
 NEXT_TICKS = 2
-UP_PIECES = 4
-DOWN_PIECES = 2
+UP_PIECES = 8
+DOWN_PIECES = 4
 PAD_ROWS = 16
 
 
@@ -1178,16 +1361,17 @@
         lax.axis_size("tp") == 4
         and count >= 4
         and count % 2 == 0
-        and gate_w.shape[0] % (16 * 2 * UP_PIECES) == 0
-        and gate_w.shape[1] % 128 == 0
-        and down_w.shape[0] % (16 * 2 * DOWN_PIECES) == 0
+        and 2 * gate_w.shape[0] % (16 * UP_PIECES) == 0
+        and gate_w.shape[1] % 256 == 128
+        and down_w.shape[0] % (16 * DOWN_PIECES) == 0
         and down_w.shape[1] % 128 == 0
-        and rows % 64 == 0
+        and rows % (2 * BLOCK) == 0
     )
 
 
 def layer(q, k, v, gates, input_log, forget_log, gain, wo, residual, norm_gain, gate_w, value_w, down_w, gate_taps, value_taps):
     count = lax.axis_size("sp")
+    line = count // 2
     heads = input_log.shape[1]
     tokens = q.shape[0]
     key_width = q.shape[1] // heads
@@ -1196,56 +1380,72 @@
     model = wo.shape[1]
     rows = residual.shape[0]
     lane = 128
-    tiles = gate_w.shape[1] // lane
+    half_width = gate_w.shape[1] // 2
+    tiles = half_width // lane
+    wide = down_w.shape[1]
+    row_pieces = 4
+    blocks = tokens // BLOCK
     logs = jnp.concatenate([input_log.T, forget_log.T], axis=0)
-    slices, wide = count, down_w.shape[1]
-    row_pieces = 4
     vmem = pl.BlockSpec(memory_space=pltpu.VMEM)
     hbm = pl.BlockSpec(memory_space=pl.ANY)
-    slots = pltpu.VMEM((slices, rows, wide), jnp.bfloat16)
+    low, full = jnp.bfloat16, jnp.float32
     dma = pltpu.SemaphoreType.DMA
     return pl.pallas_call(
         functools.partial(layer_kernel, count, heads, UP_PIECES, DOWN_PIECES),
-        out_shape=jax.ShapeDtypeStruct(residual.shape, jnp.bfloat16),
-        in_specs=[vmem] * 11 + [hbm] * 3,
+        out_shape=jax.ShapeDtypeStruct(residual.shape, low),
+        in_specs=[vmem] * 10 + [hbm] * 4,
         out_specs=vmem,
         scratch_shapes=[
-            pltpu.VMEM((tokens // BLOCK, 8, BLOCK), jnp.float32),
-            pltpu.VMEM((tokens, BLOCK), jnp.float32),
-            pltpu.VMEM((heads * span, value_width), jnp.bfloat16),
-            pltpu.VMEM((2, heads * span, value_width), jnp.bfloat16),
-            pltpu.VMEM((heads, key_width, value_width), jnp.float32),
-            pltpu.VMEM((heads, 8, key_width), jnp.float32),
-            pltpu.VMEM((heads, 8, 128), jnp.float32),
-            pltpu.VMEM((heads, key_width, value_width), jnp.float32),
-            pltpu.VMEM((heads, 8, key_width), jnp.float32),
-            pltpu.VMEM((2, heads, 8, 128), jnp.float32),
-            pltpu.VMEM((heads * span, value_width), jnp.bfloat16),
-            pltpu.VMEM((tokens, v.shape[1]), jnp.bfloat16),
-        ]
-        + [slots] * 6
-        + [
-            pltpu.VMEM((rows, model), jnp.float32),
-            pltpu.VMEM((rows, model), jnp.bfloat16),
-            pltpu.VMEM((PAD_ROWS + tokens, model), jnp.bfloat16),
-            pltpu.VMEM((tiles, model, 2 * lane), jnp.bfloat16),
-            pltpu.VMEM((count,) + down_w.shape, jnp.bfloat16),
-            pltpu.VMEM((PAD_ROWS + tokens, 2 * lane), jnp.float32),
-            pltpu.VMEM((tokens, down_w.shape[0]), jnp.bfloat16),
-            dma((2 * tiles + 1,)),
+            pltpu.VMEM((blocks, 8, BLOCK), full),
+            pltpu.VMEM((tokens, BLOCK), full),
+            pltpu.VMEM((heads * span, value_width), low),
+            pltpu.VMEM((2, heads * span, value_width), low),
+            pltpu.VMEM((heads, key_width, value_width), full),
+            pltpu.VMEM((heads, 8, key_width), full),
+            pltpu.VMEM((heads, 8, 128), full),
+            pltpu.VMEM((heads, key_width, value_width), full),
+            pltpu.VMEM((heads, 8, key_width), full),
+            pltpu.VMEM((2, heads, 8, 128), full),
+            pltpu.VMEM((heads * span, value_width), low),
+            pltpu.VMEM((tokens, v.shape[1]), low),
+            pltpu.VMEM((4, rows, v.shape[1]), low),
+            pltpu.VMEM((model, model), low),
+            pltpu.VMEM((2, gate_w.shape[0], lane), low),
+            pltpu.VMEM((gate_w.shape[0], 2 * half_width), low),
+            pltpu.VMEM((half_width, wide), low),
+            pltpu.VMEM((model, 2 * half_width), low),
+            pltpu.VMEM((count, half_width, wide), low),
+            pltpu.VMEM((rows, model), full),
+            pltpu.VMEM((rows, model), low),
+            pltpu.VMEM((PAD_ROWS + 2 * tokens, model), low),
+            pltpu.VMEM((PAD_ROWS + tokens // 2, 2 * lane), full),
+            pltpu.VMEM((2 * tokens, half_width), low),
+            pltpu.VMEM((count, 4, rows, wide), low),
+            pltpu.VMEM((count, 4, rows, wide), low),
+            pltpu.VMEM((count, 2, rows, wide), low),
+            pltpu.VMEM((count, 2, rows, wide), low),
+            pltpu.VMEM((count, rows, wide), low),
+            pltpu.VMEM((count, rows, wide), low),
+            pltpu.VMEM((count, 2, rows, wide), full),
+            dma((4 * tiles + 7,)),
+            dma((2, 3, 2)),
+            dma((2, 3)),
             dma((2,)),
             dma((2,)),
-            dma((2, UP_PIECES, count - 1)),
-            dma((2, UP_PIECES, count - 1)),
-            dma((2, DOWN_PIECES, count - 1)),
-            dma((2, DOWN_PIECES, count - 1)),
-            dma((6, slices)),
-            dma((6, slices)),
-            dma((6, row_pieces)),
+            dma((2, line - 1, UP_PIECES)),
+            dma((2, line - 1, UP_PIECES)),
+            dma((2, line - 1, DOWN_PIECES)),
+            dma((2, line - 1, DOWN_PIECES)),
+            dma((blocks,)),
+            dma((4, rows // BLOCK)),
+            dma((7, row_pieces)),
+            dma((7, row_pieces)),
+            dma((3, count)),
+            dma((3, count)),
             dma((2,)),
         ],
         compiler_params=pltpu.CompilerParams(
-            collective_id=0, has_side_effects=True, vmem_limit_bytes=60 * 1024 * 1024
+            collective_id=0, has_side_effects=True, vmem_limit_bytes=63 * 1024 * 1024
         ),
         cost_estimate=pl.CostEstimate(
             flops=30_000_000_000, bytes_accessed=8 * v.size, transcendentals=0
@@ -1257,11 +1457,11 @@
         v,
         gates,
         gain,
-        wo,
         residual,
         norm_gain[None, :],
         gate_taps,
         value_taps,
+        wo,
         gate_w,
         value_w,
         down_w,

time: 208 us -> 198 us (0.952)
  Pallas kernels: 203 us -> 191 us
    pallas_call x1, Pallas kernels: 203 us -> 191 us  [layer(): pl.pallas_call(functools.partial(layer_kernel, count, heads, UP_PIECES, D...]
where the time goes in v2:
time: 198 us; the launch traced here: 195 us
  Pallas kernels  191 us (96%)
  local copies, waits for them, and re-layouts  2.3 us (1%)
    pallas_call x1, Pallas kernels, layer(): pl.pallas_call(functools.partial(layer_kernel, count, heads, UP_PIECES, D...  191 us

profile of v2, /device:TPU:29, one launch (start us, length us, event | category | flops | bytes accessed | tf_op | source)
XLA Modules:
  0.0 194.9 jit_solution(8121704320145666418)
XLA Ops:
  0.0 0.8 fusion.2
  0.8 0.6 pad_maximum_fusion.logs_ref
  1.4 191.2 %shard_map.154 = bf16[256,2048]{1,0:T(8,128)(2,1)} custom-call(f32[4,1024]{1,0:T(4,128)} %pad_maximum_fusion.logs_ref, bf16[1024,256]{1,0:T(8,128)(2,1)} %q_ref.1, bf16[1024,256]{1,0:T(8,128)(2,1)} %k_ref.1, bf16[1024,512]{1,0:T(8,128)(2,1)} %v_ref.1, bf16[1024,512]{1,0:T(8,128)(2,1)} %gate_ref.1, f32[2,256]{1,0:T(2,128)} %gain_ref.1, ...), custom_call_target="tpu_custom_call" | custom-call | flops 30000001024 | bytes 4194304 | tf_op jit(solution)/shard_map/pallas_call | solution.py:1393
  192.6 2.3 %copy.18 = bf16[256,2048]{1,0:T(8,128)(2,1)} copy(bf16[256,2048]{1,0:T(8,128)(2,1)} %shard_map.154) | data formatting | bytes 2097152

commit v3 on v2

--- a/solution.py
+++ b/solution.py
@@ -576,6 +576,7 @@
     third_out,
     third_in,
     kept,
+    blocks_of,
     load_sem,
     wo_sem,
     give_sem,
@@ -687,12 +688,22 @@
         )
 
     give_cols = remote(give_down, full_down.at[me], give_sem.at[0, 2], give_sem.at[1, 2], sp=partner)
-    wo_step = wo_rows // 2
-
-    def wo_copy(kind, owner, p, target):
-        at = pl.multiple_of(owner * wo_rows + p * wo_step, wo_step)
+    wo_pieces = wo_sem.shape[2]
+    wo_step = wo_rows // 2 // wo_pieces
+
+    def wo_copy(kind, owner, y, s, **to):
+        at = pl.multiple_of(owner * wo_rows + (y * wo_pieces + s) * wo_step, wo_step)
         part = wo_full.at[pl.ds(at, wo_step)]
-        return remote(part, part, wo_sem.at[0, kind, p], wo_sem.at[1, kind, p], tp=target)
+        return remote(part, part, wo_sem.at[0, kind, s], wo_sem.at[1, kind, s], **to)
+
+    def wo_shard(owner):
+        part = wo_full.at[pl.ds(pl.multiple_of(owner * wo_rows, wo_rows), wo_rows)]
+        return remote(part, part, wo_sem.at[0, 0, 0], wo_sem.at[1, 0, 0], tp=near)
+
+    def wo_onward(s):
+        wo_copy(1, far, odd, s, tp=far).wait_recv()
+        wo_copy(2, far, odd, s, sp=partner).start()
+        wo_copy(3, far, odd, s, tp=near).start()
 
     def source(w, t):
         return place - t if w == 0 else place + t
@@ -714,7 +725,7 @@
 
     def down_hop(w, t, m):
         each = down_pieces // 2
-        owner = source(w, t) * 2 + lax.rem(m // each + odd, 2)
+        owner = source(w, t) * 2 + m // each
         at = lax.rem(m, each) * down_step
         part = full_down.at[owner, pl.ds(pl.multiple_of(at, down_step), down_step)]
         return remote(part, part, down_send.at[w, t, m], down_recv.at[w, t, m], sp=beyond(w))
@@ -745,7 +756,7 @@
         move(up_hop, up_pieces, n)
 
     def down_tick(n):
-        @pl.when(n == down_pieces // 2)
+        @pl.when(n == 0)
         def _():
             give_cols.wait_recv()
 
@@ -769,9 +780,9 @@
                 up_hop(w, t, lax.rem(n, up_pieces)).wait_send()
 
     give_rows(0).start()
-    for p in range(2):
-        wo_copy(0, tp, p, far).start()
-        wo_copy(1, tp, p, near).start()
+    for s in range(wo_pieces):
+        wo_copy(1, tp, odd, s, tp=far).start()
+    wo_shard(tp).start()
     for n in range(2):
         up_tick(n)
 
@@ -889,8 +900,9 @@
         )
     swap.start()
     give_rows(1).start()
-    give_cols.start()
     swap.wait_recv()
+    for s in range(wo_pieces // 2):
+        wo_onward(s)
 
     @pl.when(odd == 0)
     def _():
@@ -968,11 +980,19 @@
     def _(j):
         tick(started + j)
 
-        @pl.when(j == blocks - 2)
-        def _():
-            for p in range(2):
-                wo_copy(0, far, p, far).wait_recv()
-                wo_copy(2, far, p, near).start()
+        @pl.when(j < wo_pieces // 2)
+        def _():
+            wo_onward(wo_pieces // 2 + j)
+
+        @pl.when(j == wo_pieces // 2)
+        def _():
+            give_cols.start()
+
+        @pl.when(j >= blocks - wo_pieces)
+        def _():
+            s = j - (blocks - wo_pieces)
+            wo_copy(2, far, 1 - odd, s, sp=partner).wait_recv()
+            wo_copy(4, far, 1 - odd, s, tp=near).start()
 
         rows = pl.ds(pl.multiple_of(j * length, length), length)
         lanes = rows_ref[j]
@@ -1037,9 +1057,10 @@
             block_copy(j, tp).start()
 
     reached = started + blocks
-    for p in range(2):
-        wo_copy(1, near, p, near).wait_recv()
-        wo_copy(2, opposite, p, near).wait_recv()
+    wo_shard(near).wait_recv()
+    for s in range(wo_pieces):
+        wo_copy(3, opposite, odd, s, tp=near).wait_recv()
+        wo_copy(4, opposite, 1 - odd, s, tp=near).wait_recv()
 
     @pl.loop(0, 4)
     def _(s):
@@ -1151,6 +1172,13 @@
     parts = 4
     part_rows = tokens // parts
 
+    def ups_tick(step):
+        n = reached + step // UPS_PER_TICK
+
+        @pl.when((n < early) & (lax.rem(step, UPS_PER_TICK) == 0))
+        def _():
+            tick(n)
+
     def silu(a):
         return a * jax.nn.sigmoid(a)
 
@@ -1174,12 +1202,7 @@
 
         @pl.loop(0, tiles)
         def _(i):
-            n = reached + b * (tiles + 1) + i
-
-            @pl.when(n < early)
-            def _():
-                tick(n)
-
+            ups_tick(b * (tiles + 1) + i)
             lanes = pl.ds(pl.multiple_of(i * 2 * lane, 2 * lane), 2 * lane)
             up_tile[...] = jnp.dot(
                 group[window, :], full_up[:, lanes], preferred_element_type=jnp.float32
@@ -1190,12 +1213,7 @@
             )
             hidden[outs, pl.ds(pl.multiple_of(i * lane, lane), lane)] = act.astype(jnp.bfloat16)
 
-        n = reached + b * (tiles + 1) + tiles
-
-        @pl.when(n < early)
-        def _():
-            tick(n)
-
+        ups_tick(b * (tiles + 1) + tiles)
         up_tile[:, 0:lane] = jnp.dot(
             group[window, :], full_up[:, tail], preferred_element_type=jnp.float32
         )
@@ -1206,7 +1224,9 @@
         act = silu(both) * pltpu.roll(both, rest, 1)
         hidden[outs, tiles * lane : tiles * lane + rest] = act[:, :rest].astype(jnp.bfloat16)
 
-    @pl.loop(jnp.minimum(reached + parts * (tiles + 1), early), early)
+    ups_ticks = (parts * (tiles + 1) + UPS_PER_TICK - 1) // UPS_PER_TICK
+
+    @pl.loop(jnp.minimum(reached + ups_ticks, early), early)
     def _(n):
         tick(n)
 
@@ -1220,90 +1240,105 @@
         way = jnp.where(k <= 2 * both_sides, 1 - 2 * lax.rem(k, 2), rising)
         return place + way * away(k)
 
-    def sum_copy(stage, i, parity):
-        src, dst = ((pair_out, pair_in), (second_out, second_in), (third_out, third_in))[stage]
-        if stage == 0:
-            to = {"tp": near}
-        elif (stage == 1) == (parity == 0):
-            to = {"tp": far}
-        else:
-            to = {"sp": partner}
-        return remote(src.at[i], dst.at[i], sum_send.at[stage, i], sum_recv.at[stage, i], **to)
-
-    def term(i, y, owner):
+    def sum_copy(kind, i):
+        src, dst, to = (
+            (pair_out.at[i], pair_in.at[i], {"tp": near}),
+            (second_out.at[i, 0], second_in.at[i, 0], {"tp": far}),
+            (second_out.at[i, 1], second_in.at[i, 1], {"sp": partner}),
+            (third_out.at[i, 0], third_in.at[i, 0], {"sp": partner}),
+            (third_out.at[i, 1], third_in.at[i, 1], {"tp": far}),
+        )[kind]
+        return remote(src, dst, sum_send.at[kind, i], sum_recv.at[kind, i], **to)
+
+    part_wide = wide // 2
+    cut = (slice(0, part_wide), slice(part_wide, wide))
+
+    def term(i, a, b, side):
+        y = lax.rem(odd + a, 2)
+        x = lax.rem(chip + b, 2)
+        owner = 2 * x + lax.rem(core + side, 2)
         rows = pl.ds(pl.multiple_of((y * 4 + owner) * size, size), size)
         return jnp.dot(hidden[rows, :], full_down[i], preferred_element_type=jnp.float32)
 
-    def first_stage(i, parity):
-        for y in range(2):
-            for x in range(2):
-                pair_out[i, 2 * y + x] = term(i, y, 2 * x + 1 - core).astype(jnp.bfloat16)
-        sum_copy(0, i, parity).start()
-
-    def second_stage(i, parity):
+    def first_stage(i):
         for a in range(2):
-            y, x = (a, 1 - chip) if parity == 0 else (1 - odd, a)
-            pair_in_at = 2 * y + x
-            second_out[i, a] = term(i, y, 2 * x + core).astype(jnp.bfloat16)
+            for b in range(2):
+                pair_out[i, 2 * a + b] = term(i, a, b, 1).astype(jnp.bfloat16)
+        sum_copy(0, i).start()
         for a in range(2):
-            y, x = (a, chip) if parity == 0 else (odd, a)
-            kept[i, a] = term(i, y, 2 * x + core)
-        sum_copy(0, i, parity).wait_recv()
+            for b in range(2):
+                blocks_of[2 * a + b] = term(i, a, b, 0)
+
+    def second_stage(i):
+        sum_copy(0, i).wait_recv()
+
+        def block(a, b, side):
+            at = 2 * a + b
+            return blocks_of[at, :, cut[side]] + pair_in[i, at, :, cut[side]].astype(jnp.float32)
+
         for a in range(2):
-            y, x = (a, 1 - chip) if parity == 0 else (1 - odd, a)
-            second_out[i, a] = (
-                second_out[i, a].astype(jnp.float32) + pair_in[i, 2 * y + x].astype(jnp.float32)
+            second_out[i, 0, a] = block(a, 1, 0).astype(jnp.bfloat16)
+        sum_copy(1, i).start()
+        for b in range(2):
+            second_out[i, 1, b] = block(1, b, 1).astype(jnp.bfloat16)
+        sum_copy(2, i).start()
+        for a in range(2):
+            kept[i, 0, a] = block(a, 0, 0)
+        for b in range(2):
+            kept[i, 1, b] = block(0, b, 1)
+
+    def third_stage(i):
+        for side in range(2):
+            sum_copy(1 + side, i).wait_recv()
+            third_out[i, side] = (
+                kept[i, side, 1] + second_in[i, side, 1].astype(jnp.float32)
             ).astype(jnp.bfloat16)
-        sum_copy(1, i, parity).start()
-        for a in range(2):
-            y, x = (a, chip) if parity == 0 else (odd, a)
-            kept[i, a] += pair_in[i, 2 * y + x].astype(jnp.float32)
-
-    def third_stage(i, parity):
-        sum_copy(1, i, parity).wait_recv()
-        own = odd if parity == 0 else chip
-        third_out[i] = (kept[i, 1 - own] + second_in[i, 1 - own].astype(jnp.float32)).astype(
-            jnp.bfloat16
-        )
-        sum_copy(2, i, parity).start()
-        total_rows[:, columns(i)] = kept[i, own] + second_in[i, own].astype(jnp.float32)
-
-    def last_stage(i, parity):
-        sum_copy(2, i, parity).wait_recv()
-        cols = columns(i)
-        out_ref[:, cols] = (
-            stream[:, cols].astype(jnp.float32)
-            + (total_rows[:, cols] + third_in[i].astype(jnp.float32))
-        ).astype(out_ref.dtype)
-
-    def until(k):
-        return up_ticks + down_pieces * (jnp.maximum(away(k), 1) + 1)
-
-    @pl.loop(0, line)
-    def _(k):
-        @pl.when(k > 0)
-        def _():
-            @pl.loop(until(k - 1), until(k))
-            def _(n):
-                tick(n)
-
-        for parity in range(2):
-            first_stage(2 * unit(k) + parity, parity)
-        for parity in range(2):
-            second_stage(2 * unit(k) + parity, parity)
-
-        @pl.when(k > 0)
-        def _():
-            for parity in range(2):
-                third_stage(2 * unit(k - 1) + parity, parity)
-
-    for parity in range(2):
-        third_stage(2 * unit(line - 1) + parity, parity)
-
-    @pl.loop(0, line)
-    def _(k):
-        for parity in range(2):
-            last_stage(2 * unit(k) + parity, parity)
+            sum_copy(3 + side, i).start()
+            kept[i, side, 0] += second_in[i, side, 0].astype(jnp.float32)
+
+    def last_stage(i):
+        for side in range(2):
+            sum_copy(3 + side, i).wait_recv()
+            at = pl.multiple_of(i * wide + side * part_wide, part_wide)
+            cols = pl.ds(at, part_wide)
+            out_ref[:, cols] = (
+                stream[:, cols].astype(jnp.float32)
+                + (kept[i, side, 0] + third_in[i, side].astype(jnp.float32))
+            ).astype(out_ref.dtype)
+
+    def slice_at(n):
+        return 2 * unit(n // 2) + lax.rem(n, 2)
+
+    def due(k, j):
+        return up_ticks + down_pieces * away(k) + (j + 1) * (down_pieces // 2)
+
+    def until(n):
+        k = n // 2
+        last = jnp.where(k > 0, due(jnp.maximum(k - 1, 0), 1), early)
+        return jnp.maximum(jnp.maximum(due(k, lax.rem(n, 2)), last), early)
+
+    @pl.loop(0, count)
+    def _(n):
+        @pl.when(n > 0)
+        def _():
+            @pl.loop(until(n - 1), until(n))
+            def _(at):
+                tick(at)
+
+        first_stage(slice_at(n))
+
+        @pl.when(n > 1)
+        def _():
+            third_stage(slice_at(n - 2))
+
+        second_stage(slice_at(n))
+
+    for n in (count - 2, count - 1):
+        third_stage(slice_at(n))
+
+    @pl.loop(0, count)
+    def _(n):
+        last_stage(slice_at(n))
 
     swap.wait_send()
 
@@ -1314,8 +1349,10 @@
 
     for p in range(2):
         give_rows(p).wait_send()
-        for kind in range(3):
-            wo_copy(kind, tp, p, near).wait_send()
+    wo_shard(tp).wait_send()
+    for s in range(wo_pieces):
+        for kind in range(1, 5):
+            wo_copy(kind, tp, 0, s, tp=near).wait_send()
     give_cols.wait_send()
 
     @pl.loop(0, blocks)
@@ -1331,8 +1368,8 @@
 
     @pl.loop(0, count)
     def _(i):
-        for stage in range(3):
-            sum_copy(stage, i, 0).wait_send()
+        for kind in range(5):
+            sum_copy(kind, i).wait_send()
 
     @pl.loop(started - 2, up_ticks)
     def _(n):
@@ -1350,6 +1387,7 @@
 
 FIRST_TICKS = 4
 NEXT_TICKS = 2
+UPS_PER_TICK = 4
 UP_PIECES = 8
 DOWN_PIECES = 4
 PAD_ROWS = 16
@@ -1364,8 +1402,9 @@
         and 2 * gate_w.shape[0] % (16 * UP_PIECES) == 0
         and gate_w.shape[1] % 256 == 128
         and down_w.shape[0] % (16 * DOWN_PIECES) == 0
-        and down_w.shape[1] % 128 == 0
+        and down_w.shape[1] % 256 == 0
         and rows % (2 * BLOCK) == 0
+        and 4 * rows >= 6 * BLOCK
     )
 
 
@@ -1422,13 +1461,14 @@
             pltpu.VMEM((2 * tokens, half_width), low),
             pltpu.VMEM((count, 4, rows, wide), low),
             pltpu.VMEM((count, 4, rows, wide), low),
-            pltpu.VMEM((count, 2, rows, wide), low),
-            pltpu.VMEM((count, 2, rows, wide), low),
-            pltpu.VMEM((count, rows, wide), low),
-            pltpu.VMEM((count, rows, wide), low),
-            pltpu.VMEM((count, 2, rows, wide), full),
+            pltpu.VMEM((count, 2, 2, rows, wide // 2), low),
+            pltpu.VMEM((count, 2, 2, rows, wide // 2), low),
+            pltpu.VMEM((count, 2, rows, wide // 2), low),
+            pltpu.VMEM((count, 2, rows, wide // 2), low),
+            pltpu.VMEM((count, 2, 2, rows, wide // 2), full),
+            pltpu.VMEM((4, rows, wide), full),
             dma((4 * tiles + 7,)),
-            dma((2, 3, 2)),
+            dma((2, 5, 4)),
             dma((2, 3)),
             dma((2,)),
             dma((2,)),
@@ -1440,8 +1480,8 @@
             dma((4, rows // BLOCK)),
             dma((7, row_pieces)),
             dma((7, row_pieces)),
-            dma((3, count)),
-            dma((3, count)),
+            dma((5, count)),
+            dma((5, count)),
             dma((2,)),
         ],
         compiler_params=pltpu.CompilerParams(

time: 198 us -> 180 us (0.909); the launches traced: 195 us -> 179 us
  Pallas kernels: 191 us -> 176 us
    pallas_call x1, Pallas kernels: 191 us -> 176 us  [layer(): pl.pallas_call(functools.partial(layer_kernel, count, heads, UP_PIECES, D...]
where the time goes in v3:
time: 180 us; the launch traced here: 179 us
  Pallas kernels  176 us (98%)
  local copies, waits for them, and re-layouts  2.3 us (1%)
    pallas_call x1, Pallas kernels, layer(): pl.pallas_call(functools.partial(layer_kernel, count, heads, UP_PIECES, D...  176 us

profile of v3, /device:TPU:29, one launch (start us, length us, event | category | flops | bytes accessed | tf_op | source)
XLA Modules:
  0.0 179.2 jit_solution(8149487080454067835)
XLA Ops:
  0.0 0.8 fusion.2
  0.8 0.6 pad_maximum_fusion.logs_ref
  1.4 175.5 %shard_map.154 = bf16[256,2048]{1,0:T(8,128)(2,1)} custom-call(f32[4,1024]{1,0:T(4,128)} %pad_maximum_fusion.logs_ref, bf16[1024,256]{1,0:T(8,128)(2,1)} %q_ref.1, bf16[1024,256]{1,0:T(8,128)(2,1)} %k_ref.1, bf16[1024,512]{1,0:T(8,128)(2,1)} %v_ref.1, bf16[1024,512]{1,0:T(8,128)(2,1)} %gate_ref.1, f32[2,256]{1,0:T(2,128)} %gain_ref.1, ...), custom_call_target="tpu_custom_call" | custom-call | flops 30000001024 | bytes 4194304 | tf_op jit(solution)/shard_map/pallas_call | solution.py:1432
  176.9 2.3 %copy.18 = bf16[256,2048]{1,0:T(8,128)(2,1)} copy(bf16[256,2048]{1,0:T(8,128)(2,1)} %shard_map.154) | data formatting | bytes 2097152

commit v4 on v3

--- a/solution.py
+++ b/solution.py
@@ -531,20 +531,25 @@
     up_pieces,
     down_pieces,
     logs_ref,
-    q_ref,
-    k_ref,
-    v_ref,
-    gate_ref,
     gain_ref,
-    residual_ref,
     norm_gain_ref,
     gate_taps_ref,
     value_taps_ref,
+    q_hbm,
+    k_hbm,
+    v_hbm,
+    gate_hbm,
+    residual_hbm,
     wo_ref,
     gate_w_ref,
     value_w_ref,
     down_w_ref,
     out_ref,
+    q_ref,
+    k_ref,
+    v_ref,
+    gate_ref,
+    residual_ref,
     rows_ref,
     cols_ref,
     state_ref,
@@ -568,6 +573,7 @@
     stream,
     group,
     up_tile,
+    up_other,
     hidden,
     pair_out,
     pair_in,
@@ -638,16 +644,24 @@
                 load(w_ref.at[:, pl.ds(at, lane)], to)
     for a, w_ref in enumerate((gate_w_ref, value_w_ref)):
         load(w_ref.at[:, pl.ds(tiles * lane, lane)], middle.at[a])
+    first_loads = len(loads)
+    load(k_hbm, k_ref)
+    load(v_hbm, v_ref)
+    load(wo_ref, wo_full.at[wo_own])
+    soon_loads = len(loads)
     for to, y in ((full_down.at[me], odd), (give_down, 1 - odd)):
         at = pl.multiple_of(y * shift, rest)
         load(down_w_ref.at[pl.ds(at, tiles * lane)], to.at[pl.ds(0, tiles * lane)])
         at = pl.multiple_of(tiles * lane + y * rest, rest)
         load(down_w_ref.at[pl.ds(at, rest)], to.at[pl.ds(tiles * lane, rest)])
-    load(wo_ref, wo_full.at[wo_own])
-    for one in loads:
+    load(q_hbm, q_ref)
+    load(gate_hbm, gate_ref)
+    load(residual_hbm, residual_ref)
+    for one in loads[:first_loads]:
         one.start()
-    pl.semaphore_wait(barrier, 6)
-    for one in loads:
+    for one in loads[first_loads:]:
+        one.start()
+    for one in loads[:first_loads]:
         one.wait()
 
     def remote(src, dst, send_sem, recv_sem, **to):
@@ -733,16 +747,21 @@
     up_ticks = line * up_pieces
     all_ticks = up_ticks + line * down_pieces
 
+    at_end = (place == 0) | (place == line - 1)
+
     def move(hop, pieces, n):
         t = n // pieces
         m = lax.rem(n, pieces)
         for w in range(2):
+            due = sends(w, t)
+            if hop is down_hop:
+                due = due & ((t > 0) | jnp.logical_not(at_end))
 
             @pl.when(has(w, t) & (t > 0))
             def _():
                 hop(w, t - 1, m).wait_recv()
 
-            @pl.when(sends(w, t))
+            @pl.when(due)
             def _():
                 hop(w, t, m).start()
 
@@ -756,20 +775,25 @@
         move(up_hop, up_pieces, n)
 
     def down_tick(n):
-        @pl.when(n == 0)
+        @pl.when((n == 0) & jnp.logical_not(at_end))
         def _():
             give_cols.wait_recv()
 
         move(down_hop, down_pieces, n)
 
+    def late_tick(n):
+        @pl.when((n >= up_ticks) & (n < all_ticks))
+        def _():
+            down_tick(n - up_ticks)
+
     def tick(n):
-        @pl.when(n < up_ticks)
-        def _():
-            up_tick(n)
-
-        @pl.when((n >= up_ticks) & (n < all_ticks))
-        def _():
-            down_tick(n - up_ticks)
+        @pl.when((n < up_pieces) | jnp.logical_not(at_end))
+        def _():
+            @pl.when(n < up_ticks)
+            def _():
+                up_tick(n)
+
+            late_tick(n)
 
     def up_sent(n):
         t = n // up_pieces
@@ -779,12 +803,15 @@
             def _():
                 up_hop(w, t, lax.rem(n, up_pieces)).wait_send()
 
+    pl.semaphore_wait(barrier, 6)
+    for n in range(2):
+        up_tick(n)
     give_rows(0).start()
+    for one in loads[first_loads:soon_loads]:
+        one.wait()
     for s in range(wo_pieces):
         wo_copy(1, tp, odd, s, tp=far).start()
     wo_shard(tp).start()
-    for n in range(2):
-        up_tick(n)
 
     key_width = memory.shape[1]
     value_width = memory.shape[2]
@@ -900,6 +927,8 @@
         )
     swap.start()
     give_rows(1).start()
+    for one in loads[soon_loads:]:
+        one.wait()
     swap.wait_recv()
     for s in range(wo_pieces // 2):
         wo_onward(s)
@@ -922,7 +951,7 @@
             keep((pair_memory, pair_normer, pair_level.at[0]), h, out)
             pair_level[1, h] = jnp.broadcast_to(total_a + total_b, pair_level.shape[2:])
 
-    started = jnp.minimum(FIRST_TICKS + NEXT_TICKS * place, up_ticks)
+    started = jnp.minimum(FIRST_TICKS + NEXT_TICKS * place, jnp.where(at_end, up_pieces, up_ticks))
 
     @pl.loop(2, started)
     def _(n):
@@ -1073,6 +1102,16 @@
 
     reached = reached + 4
 
+    @pl.when(at_end)
+    def _():
+        give_cols.wait_recv()
+        for w in range(2):
+
+            @pl.when(sends(w, 0))
+            def _():
+                for m in range(down_pieces):
+                    down_hop(w, 0, m).start()
+
     def columns(i):
         return pl.ds(pl.multiple_of(i * wide, wide), wide)
 
@@ -1163,21 +1202,15 @@
     def _():
         edge.start()
 
-    @pl.loop(jnp.minimum(reached, up_ticks), up_ticks)
+    @pl.loop(jnp.where(at_end, up_pieces, jnp.minimum(reached, up_ticks)), up_ticks)
     def _(n):
         up_tick(n)
 
     reached = jnp.maximum(reached, up_ticks)
-    early = up_ticks + 2 * down_pieces
+    early = up_ticks + jnp.where(at_end, 1, 2) * down_pieces
     parts = 4
+    up_tiles = (up_tile, up_other)
     part_rows = tokens // parts
-
-    def ups_tick(step):
-        n = reached + step // UPS_PER_TICK
-
-        @pl.when((n < early) & (lax.rem(step, UPS_PER_TICK) == 0))
-        def _():
-            tick(n)
 
     def silu(a):
         return a * jax.nn.sigmoid(a)
@@ -1193,40 +1226,58 @@
         def _():
             edge.wait_recv()
 
-        def conv(taps, width):
+        for m in range(UPS_TICKS):
+            n = reached + b * UPS_TICKS + m
+
+            @pl.when(n < early)
+            def _():
+                tick(n)
+
+        def conv(ref, taps, width):
             return (
-                taps[0:1, :] * up_tile[pad - 2 : pad - 2 + part_rows, width]
-                + taps[1:2, :] * up_tile[pad - 1 : pad - 1 + part_rows, width]
-                + taps[2:3, :] * up_tile[pad : pad + part_rows, width]
+                taps[0:1, :] * ref[pad - 2 : pad - 2 + part_rows, width]
+                + taps[1:2, :] * ref[pad - 1 : pad - 1 + part_rows, width]
+                + taps[2:3, :] * ref[pad : pad + part_rows, width]
             )
 
-        @pl.loop(0, tiles)
-        def _(i):
-            ups_tick(b * (tiles + 1) + i)
-            lanes = pl.ds(pl.multiple_of(i * 2 * lane, 2 * lane), 2 * lane)
-            up_tile[...] = jnp.dot(
-                group[window, :], full_up[:, lanes], preferred_element_type=jnp.float32
-            )
-            taps_at = pl.ds(pl.multiple_of(odd * shift + i * lane, lane), lane)
-            act = silu(conv(gate_taps_ref[:, taps_at], slice(0, lane))) * conv(
-                value_taps_ref[:, taps_at], slice(lane, 2 * lane)
-            )
-            hidden[outs, pl.ds(pl.multiple_of(i * lane, lane), lane)] = act.astype(jnp.bfloat16)
-
-        ups_tick(b * (tiles + 1) + tiles)
-        up_tile[:, 0:lane] = jnp.dot(
-            group[window, :], full_up[:, tail], preferred_element_type=jnp.float32
-        )
-        mid = slice(tiles * lane, (tiles + 1) * lane)
-        low = lax.broadcasted_iota(jnp.int32, (3, lane), 1) < rest
-        taps_a, taps_b = halves_of(gate_taps_ref[:, mid], value_taps_ref[:, mid], low)
-        both = conv(jnp.where(odd == 0, taps_a, taps_b), slice(0, lane))
-        act = silu(both) * pltpu.roll(both, rest, 1)
-        hidden[outs, tiles * lane : tiles * lane + rest] = act[:, :rest].astype(jnp.bfloat16)
-
-    ups_ticks = (parts * (tiles + 1) + UPS_PER_TICK - 1) // UPS_PER_TICK
-
-    @pl.loop(jnp.minimum(reached + ups_ticks, early), early)
+        def product(i):
+            ref = up_tiles[i % 2]
+            if i < tiles:
+                ref[...] = jnp.dot(
+                    group[window, :],
+                    full_up[:, 2 * i * lane : 2 * (i + 1) * lane],
+                    preferred_element_type=jnp.float32,
+                )
+            else:
+                ref[:, 0:lane] = jnp.dot(
+                    group[window, :], full_up[:, tail], preferred_element_type=jnp.float32
+                )
+
+        def finish(i):
+            ref = up_tiles[i % 2]
+            if i < tiles:
+                taps_at = pl.ds(pl.multiple_of(odd * shift + i * lane, lane), lane)
+                act = silu(conv(ref, gate_taps_ref[:, taps_at], slice(0, lane))) * conv(
+                    ref, value_taps_ref[:, taps_at], slice(lane, 2 * lane)
+                )
+                hidden[outs, i * lane : (i + 1) * lane] = act.astype(jnp.bfloat16)
+            else:
+                mid = slice(tiles * lane, (tiles + 1) * lane)
+                low = lax.broadcasted_iota(jnp.int32, (3, lane), 1) < rest
+                taps_a, taps_b = halves_of(gate_taps_ref[:, mid], value_taps_ref[:, mid], low)
+                both = conv(ref, jnp.where(odd == 0, taps_a, taps_b), slice(0, lane))
+                act = silu(both) * pltpu.roll(both, rest, 1)
+                hidden[outs, tiles * lane : tiles * lane + rest] = act[:, :rest].astype(
+                    jnp.bfloat16
+                )
+
+        product(0)
+        for i in range(tiles):
+            product(i + 1)
+            finish(i)
+        finish(tiles)
+
+    @pl.loop(jnp.minimum(reached + parts * UPS_TICKS, early), early)
     def _(n):
         tick(n)
 
@@ -1323,7 +1374,7 @@
         def _():
             @pl.loop(until(n - 1), until(n))
             def _(at):
-                tick(at)
+                late_tick(at)
 
         first_stage(slice_at(n))
 
@@ -1387,7 +1438,7 @@
 
 FIRST_TICKS = 4
 NEXT_TICKS = 2
-UPS_PER_TICK = 4
+UPS_TICKS = 1
 UP_PIECES = 8
 DOWN_PIECES = 4
 PAD_ROWS = 16
@@ -1432,9 +1483,14 @@
     return pl.pallas_call(
         functools.partial(layer_kernel, count, heads, UP_PIECES, DOWN_PIECES),
         out_shape=jax.ShapeDtypeStruct(residual.shape, low),
-        in_specs=[vmem] * 10 + [hbm] * 4,
+        in_specs=[vmem] * 5 + [hbm] * 9,
         out_specs=vmem,
         scratch_shapes=[
+            pltpu.VMEM(q.shape, low),
+            pltpu.VMEM(k.shape, low),
+            pltpu.VMEM(v.shape, low),
+            pltpu.VMEM(gates.shape, low),
+            pltpu.VMEM(residual.shape, low),
             pltpu.VMEM((blocks, 8, BLOCK), full),
             pltpu.VMEM((tokens, BLOCK), full),
             pltpu.VMEM((heads * span, value_width), low),
@@ -1458,6 +1514,7 @@
             pltpu.VMEM((rows, model), low),
             pltpu.VMEM((PAD_ROWS + 2 * tokens, model), low),
             pltpu.VMEM((PAD_ROWS + tokens // 2, 2 * lane), full),
+            pltpu.VMEM((PAD_ROWS + tokens // 2, 2 * lane), full),
             pltpu.VMEM((2 * tokens, half_width), low),
             pltpu.VMEM((count, 4, rows, wide), low),
             pltpu.VMEM((count, 4, rows, wide), low),
@@ -1467,7 +1524,7 @@
             pltpu.VMEM((count, 2, rows, wide // 2), low),
             pltpu.VMEM((count, 2, 2, rows, wide // 2), full),
             pltpu.VMEM((4, rows, wide), full),
-            dma((4 * tiles + 7,)),
+            dma((4 * tiles + 12,)),
             dma((2, 5, 4)),
             dma((2, 3)),
             dma((2,)),
@@ -1492,15 +1549,15 @@
         ),
     )(
         logs,
+        gain,
+        norm_gain[None, :],
+        gate_taps,
+        value_taps,
         q,
         k,
         v,
         gates,
-        gain,
         residual,
-        norm_gain[None, :],
-        gate_taps,
-        value_taps,
         wo,
         gate_w,
         value_w,

time: 180 us -> 174 us (0.967)
  Pallas kernels: 176 us -> 169 us
    pallas_call x1, Pallas kernels: 176 us -> 169 us  [layer(): pl.pallas_call(functools.partial(layer_kernel, count, heads, UP_PIECES, D...]
where the time goes in v4:
time: 174 us; the launch traced here: 172 us
  Pallas kernels  169 us (97%)
  local copies, waits for them, and re-layouts  2.3 us (1%)
    pallas_call x1, Pallas kernels, layer(): pl.pallas_call(functools.partial(layer_kernel, count, heads, UP_PIECES, D...  169 us

profile of v4, /device:TPU:29, one launch (start us, length us, event | category | flops | bytes accessed | tf_op | source)
XLA Modules:
  0.0 172.4 jit_solution(5145542670311476259)
XLA Ops:
  0.0 0.8 fusion.2
  0.8 0.6 pad_maximum_fusion.logs_ref
  1.4 168.7 %shard_map.154 = bf16[256,2048]{1,0:T(8,128)(2,1)} custom-call(f32[4,1024]{1,0:T(4,128)} %pad_maximum_fusion.logs_ref, f32[2,256]{1,0:T(2,128)} %gain_ref.1, f32[1,2048]{1,0:T(1,128)} %bitcast.5, f32[3,1408]{1,0:T(4,128)} %gate_taps_ref.1, f32[3,1408]{1,0:T(4,128)} %value_taps_ref.1, bf16[1024,256]{1,0:T(8,128)(2,1)} %q_hbm.1, bf16[1024,256]{1,0:T(8,128)(2,1)} %k_hbm.1, ...), custom_call_target="tpu_custom_call" | custom-call | flops 30000001024 | bytes 4194304 | tf_op jit(solution)/shard_map/pallas_call | solution.py:1483
  170.1 2.3 %copy.18 = bf16[256,2048]{1,0:T(8,128)(2,1)} copy(bf16[256,2048]{1,0:T(8,128)(2,1)} %shard_map.154) | data formatting | bytes 2097152

commit v5 on v4

--- a/solution.py
+++ b/solution.py
@@ -530,7 +530,8 @@
     heads,
     up_pieces,
     down_pieces,
-    logs_ref,
+    input_logs_ref,
+    forget_logs_ref,
     gain_ref,
     norm_gain_ref,
     gate_taps_ref,
@@ -599,6 +600,7 @@
     sum_send,
     sum_recv,
     edge_sem,
+    out_sem,
 ):
     me = lax.axis_index("sp")
     tp = lax.axis_index("tp")
@@ -860,22 +862,22 @@
     at_row = lax.broadcasted_iota(jnp.int32, (length, length), 0)
     at_col = lax.broadcasted_iota(jnp.int32, (length, length), 1)
 
-    def by_block(first):
+    def by_block(ref):
         return jnp.concatenate(
             [
-                logs_ref[first : first + heads, b * length : (b + 1) * length]
+                ref[:, b * length : (b + 1) * length]
                 for b in range(blocks)
             ],
             axis=0,
         )
 
     within = jnp.dot(
-        by_block(heads),
+        by_block(forget_logs_ref),
         jnp.where(at_row <= at_col, 1.0, 0.0),
         precision=lax.Precision.HIGHEST,
         preferred_element_type=jnp.float32,
     )
-    shifted_all = by_block(0) - within
+    shifted_all = by_block(input_logs_ref) - within
     each_all = within[:, length - 1 : length]
     after = jnp.zeros((heads, 1), jnp.float32)
     to_end = [None] * blocks
@@ -1347,15 +1349,21 @@
             sum_copy(3 + side, i).start()
             kept[i, side, 0] += second_in[i, side, 0].astype(jnp.float32)
 
+    def out_copy(i):
+        return pltpu.make_async_copy(
+            stream.at[:, columns(i)], out_ref.at[:, columns(i)], out_sem.at[i]
+        )
+
     def last_stage(i):
         for side in range(2):
             sum_copy(3 + side, i).wait_recv()
             at = pl.multiple_of(i * wide + side * part_wide, part_wide)
             cols = pl.ds(at, part_wide)
-            out_ref[:, cols] = (
+            stream[:, cols] = (
                 stream[:, cols].astype(jnp.float32)
                 + (kept[i, side, 0] + third_in[i, side].astype(jnp.float32))
-            ).astype(out_ref.dtype)
+            ).astype(stream.dtype)
+        out_copy(i).start()
 
     def slice_at(n):
         return 2 * unit(n // 2) + lax.rem(n, 2)
@@ -1384,12 +1392,20 @@
 
         second_stage(slice_at(n))
 
-    for n in (count - 2, count - 1):
-        third_stage(slice_at(n))
+        @pl.when(n > 3)
+        def _():
+            last_stage(slice_at(n - 4))
+
+    third_stage(slice_at(count - 2))
+    last_stage(slice_at(count - 4))
+    last_stage(slice_at(count - 3))
+    third_stage(slice_at(count - 1))
+    last_stage(slice_at(count - 2))
+    last_stage(slice_at(count - 1))
 
     @pl.loop(0, count)
     def _(n):
-        last_stage(slice_at(n))
+        out_copy(n).wait()
 
     swap.wait_send()
 
@@ -1475,7 +1491,6 @@
     wide = down_w.shape[1]
     row_pieces = 4
     blocks = tokens // BLOCK
-    logs = jnp.concatenate([input_log.T, forget_log.T], axis=0)
     vmem = pl.BlockSpec(memory_space=pltpu.VMEM)
     hbm = pl.BlockSpec(memory_space=pl.ANY)
     low, full = jnp.bfloat16, jnp.float32
@@ -1483,8 +1498,8 @@
     return pl.pallas_call(
         functools.partial(layer_kernel, count, heads, UP_PIECES, DOWN_PIECES),
         out_shape=jax.ShapeDtypeStruct(residual.shape, low),
-        in_specs=[vmem] * 5 + [hbm] * 9,
-        out_specs=vmem,
+        in_specs=[vmem] * 6 + [hbm] * 9,
+        out_specs=hbm,
         scratch_shapes=[
             pltpu.VMEM(q.shape, low),
             pltpu.VMEM(k.shape, low),
@@ -1540,6 +1555,7 @@
             dma((5, count)),
             dma((5, count)),
             dma((2,)),
+            dma((count,)),
         ],
         compiler_params=pltpu.CompilerParams(
             collective_id=0, has_side_effects=True, vmem_limit_bytes=63 * 1024 * 1024
@@ -1548,7 +1564,8 @@
             flops=30_000_000_000, bytes_accessed=8 * v.size, transcendentals=0
         ),
     )(
-        logs,
+        input_log.T,
+        forget_log.T,
         gain,
         norm_gain[None, :],
         gate_taps,

time: 174 us -> 173 us (level)
  no operation moved by 1% of the time
where the time goes in v5:
time: 173 us; the launch traced here: 172 us
  Pallas kernels  168 us (97%)
  local copies, waits for them, and re-layouts  2.3 us (1%)
    pallas_call x1, Pallas kernels, layer(): pl.pallas_call(functools.partial(layer_kernel, count, heads, UP_PIECES, D...  168 us

profile of v5, /device:TPU:29, one launch (start us, length us, event | category | flops | bytes accessed | tf_op | source)
XLA Modules:
  0.0 172.1 jit_solution(4134027525371611409)
XLA Ops:
  0.0 1.4 fusion.2
  1.4 168.5 %shard_map.154 = bf16[256,2048]{1,0:T(8,128)(2,1)} custom-call(f32[2,1024]{1,0:T(2,128)} %get-tuple-element.6.input_logs_ref, f32[2,1024]{1,0:T(2,128)} %get-tuple-element.5.forget_logs_ref, f32[2,256]{1,0:T(2,128)} %gain_ref.1, f32[1,2048]{1,0:T(1,128)} %bitcast.5, f32[3,1408]{1,0:T(4,128)} %gate_taps_ref.1, f32[3,1408]{1,0:T(4,128)} %value_taps_ref.1, ...), custom_call_target="tpu_custom_call" | custom-call | flops 30000001024 | bytes 4194304 | tf_op jit(solution)/shard_map/pallas_call | solution.py:1498
  169.8 2.3 %copy.18 = bf16[256,2048]{1,0:T(8,128)(2,1)} copy(bf16[256,2048]{1,0:T(8,128)(2,1)} %shard_map.154) | data formatting | bytes 2097152
